TPU v7x, 32 devices: a whole 2x2x4 slice. The times are simulated.
32 devices in a mesh: sp: 8 (over z, y), tp: 4 (over x, core).
Axes of the slice: x: 2, y: 2, z: 4, core: 2. Of those that a mesh axis runs over, the one named last changes fastest.
Arguments:
- block_input: bfloat16 [8192, 2048], P('sp'), may hold values from -6 to 6
- out_grad: bfloat16 [8192, 2048], P('sp'), may hold values from -6 to 6
- w_value: bfloat16 [2048, 1024], P(None, 'tp'), may hold values from -0.125 to 0.125
- w_gate: bfloat16 [2048, 1024], P(None, 'tp'), may hold values from -0.125 to 0.125
- conv_taps: float32 [31, 1024], P(None, 'tp'), may hold values from -4 to 4
- norm_gain: float32 [1024], P('tp'), may hold values from 0.1 to 1.9
- norm_shift: float32 [1024], P('tp'), may hold values from -3 to 3
- w_proj: bfloat16 [1024, 2048], P('tp'), may hold values from -0.1875 to 0.1875
Outputs:
- input_grad: bfloat16 [8192, 2048], P('sp', 'tp')
- value_wgrad: float32 [2048, 1024], P('sp', 'tp')
- gate_wgrad: float32 [2048, 1024], P('sp', 'tp')
- proj_wgrad: float32 [1024, 2048], P('tp', 'sp')
- taps_grad: float32 [31, 1024], P(None, 'tp')
- gain_grad: float32 [1024], P('tp')
- shift_grad: float32 [1024], P('tp')
All inputs are finite; a program needn't handle non-finite values.
Results may differ from a plain program's by a relative error of at most 0.014.
Values may be sent and summed in bfloat16 or wider, within the bound.
A program may use at most 128 MiB of HBM per device.

v0:
```python
import functools
import math

import jax
import jax.numpy as jnp
from jax import lax
from jax.experimental import pallas as pl
from jax.experimental.pallas import tpu as pltpu
from jax.sharding import PartitionSpec as P

CH = 1024


EPS = 0.05


def from_behind(block, axis, distance):
    devices = range(lax.axis_size(axis))
    route = [(i - distance, i) for i in devices if i - distance in devices]
    return lax.ppermute(block, axis, route)


def right_product(left, right):
    return lax.dot_general(
        left, right, (((1,), (1,)), ((), ())), preferred_element_type=jnp.float32
    )


def column_product(left, right):
    return lax.dot_general(
        left, right, (((0,), (0,)), ((), ())), preferred_element_type=jnp.float32
    )


MESH = pl.DeviceIdType.MESH


def tail_kernel(
    n, n_tp, loss_scale,
    bi_hbm, og_hbm, wv_hbm, wg_hbm, gb_ref, mo_ref, small_ref,
    ig_ref, ws_ref, ps_ref, sm_ref,
    bi, og, wv, wg,
    gs, gr, gs2, gq, pm, pr, ps2, pq,
    xs, xr, ys, yr, acc, small_pair, small_in, small_all,
    load_sem,
    gs_send, gs_recv, gq_send, gq_recv, pr_send, pr_recv, pq_send, pq_recv,
    x_send, x_recv, y_send, y_recv, s_send, s_recv, sa_send, sa_recv,
):
    me, t = lax.axis_index("sp"), lax.axis_index("tp")
    outer, inner = me // 2, me % 2
    h = n // 2
    mate = 2 * outer + (1 - inner)
    t_near, t_far = t + 1 - 2 * (t % 2), lax.rem(t + n_tp // 2, n_tp)
    t_cross = lax.rem(t_near + n_tp // 2, n_tp)
    rows = bi.shape[1] // n
    tokens = bi.shape[0]
    cols = bi.shape[1] // n_tp
    chans = mo_ref.shape[1]
    chunks = xs.shape[0]
    step = tokens // chunks

    loads = []
    for i, (src, dst) in enumerate(((bi_hbm, bi), (wv_hbm, wv), (wg_hbm, wg), (og_hbm, og))):
        loads.append(pltpu.make_async_copy(src, dst, load_sem.at[i]))
        loads[-1].start()

    barrier = pltpu.get_barrier_semaphore()
    peers = [{"sp": 2 * lax.rem(outer + k, h) + inner} for k in range(1, h)]
    for who in peers + [{"sp": mate}, {"tp": t_near}, {"tp": t_far}]:
        pl.semaphore_signal(barrier, inc=1, device_id=who, device_id_type=MESH)
    pl.semaphore_wait(barrier, len(peers) + 3)

    def send(src, dst, send_sem, recv_sem, who):
        copy = pltpu.make_async_remote_copy(
            src_ref=src, dst_ref=dst, send_sem=send_sem, recv_sem=recv_sem,
            device_id=who, device_id_type=MESH,
        )
        copy.start()
        return copy

    small_copy = send(small_ref, small_in, s_send.at[0], s_recv.at[0], {"sp": mate})

    aligned = rows % 128 == 0
    wide = 256
    def block_rows(o, i):
        return pl.ds(pl.multiple_of((2 * o + i) * rows, rows), rows)

    def product(act, other, where):
        return lax.dot_general(
            act[:, where], other[...], (((0,), (0,)), ((), ())),
            preferred_element_type=jnp.float32,
        ).astype(jnp.bfloat16)

    def make_block(store, act, other, o, i):
        if aligned:
            store[block_rows(o, i), :] = product(act, other, block_rows(o, i))

    def make_all(store, act, other):
        if not aligned:
            for c in range(act.shape[1] // wide):
                where = pl.ds(c * wide, wide)
                store[where, :] = product(act, other, where)

    def partial_input(r, j):
        at = pl.ds(pl.multiple_of(j * cols, cols), cols)
        token = pl.ds(r * step, step)
        return right_product(gb_ref[token, :chans], wv[at, :]) + right_product(
            gb_ref[token, chans:], wg[at, :]
        )

    order = [lax.rem(outer + k, h) for k in range(1, h)] + [outer]

    def near_block(r):
        xs[r, 0] = partial_input(r, t_near).astype(jnp.bfloat16)
        xs[r, 1] = partial_input(r, t_cross).astype(jnp.bfloat16)
        return send(xs.at[r], xr.at[r], x_send.at[r], x_recv.at[r], {"tp": t_near})

    def far_block(r):
        mine = partial_input(r, t)
        far = partial_input(r, t_far)
        x_copies[r].wait_recv()
        ys[r] = (far + xr[r, 1].astype(jnp.float32)).astype(jnp.bfloat16)
        acc[pl.ds(r * step, step), :] = mine + xr[r, 0].astype(jnp.float32)
        return send(ys.at[r], yr.at[r], y_send.at[r], y_recv.at[r], {"tp": t_far})

    loads[0].wait()
    make_all(gs, bi, gb_ref)
    g_copies = []
    x_copies = []
    y_copies = []

    def g_block(k):
        o = order[k]
        make_block(gs, bi, gb_ref, o, 1 - inner)
        where = block_rows(o, 1 - inner)
        g_copies.append(send(gs.at[where], gr.at[k], gs_send.at[k], gs_recv.at[k], {"sp": mate}))

    g_block(0)
    loads[1].wait()
    loads[2].wait()
    x_copies.append(near_block(0))
    g_block(1)
    x_copies.append(near_block(1))
    y_copies.append(far_block(0))
    loads[3].wait()
    make_all(pm, og, mo_ref)
    p_copies = []
    for k in range(h - 1):
        o = order[k]
        for i in range(2):
            make_block(pm, og, mo_ref, o, i)
        where = pl.ds(pl.multiple_of(2 * o * rows, 2 * rows), 2 * rows)
        p_copies.append(send(pm.at[where], pr.at[k], pr_send.at[k], pr_recv.at[k], {"sp": 2 * o + inner}))
        if k + 2 < h:
            g_block(k + 2)
    for r in range(2, chunks):
        x_copies.append(near_block(r))
        y_copies.append(far_block(r - 1))
    y_copies.append(far_block(chunks - 1))
    for i in range(2):
        make_block(pm, og, mo_ref, outer, i)
    small_copy.wait()
    small_pair[...] = small_ref[...] + small_in[...]
    sa_copies = [
        send(small_pair, small_all.at[outer], sa_send.at[k - 1], sa_recv.at[k - 1],
             {"sp": 2 * lax.rem(outer + k, h) + inner})
        for k in range(1, h)
    ]
    q_copies = []
    for k in range(h):
        o = order[k]
        make_block(gs, bi, gb_ref, o, inner)
        g_copies[k].wait_recv()
        total = gs[block_rows(o, inner), :].astype(jnp.float32) + gr[k].astype(jnp.float32)
        if k < h - 1:
            gs2[k] = total.astype(jnp.bfloat16)
            q_copies.append(send(gs2.at[k], gq.at[k], gq_send.at[k], gq_recv.at[k], {"sp": 2 * o + inner}))
        else:
            ws_ref[...] = total
    for copy in p_copies:
        copy.wait_recv()

    def proj_total(i):
        total = pm[block_rows(outer, i), :].astype(jnp.float32)
        for k in range(h - 1):
            total = total + pr[k, pl.ds(pl.multiple_of(i * rows, rows), rows), :].astype(jnp.float32)
        return total

    ps2[...] = proj_total(1 - inner).astype(jnp.bfloat16)
    last = send(ps2, pq, pq_send.at[0], pq_recv.at[0], {"sp": mate})
    ps_ref[...] = proj_total(inner)
    for copy in sa_copies:
        copy.wait_recv()
    small_all[outer] = small_pair[...]
    total = small_all[0]
    for k in range(1, h):
        total = total + small_all[k]
    sm_ref[...] = total * loss_scale
    for r in range(chunks):
        y_copies[r].wait_recv()
        token = pl.ds(r * step, step)
        ig_ref[token, :] = (acc[token, :] + yr[r].astype(jnp.float32)).astype(jnp.bfloat16)
    for copy in q_copies:
        copy.wait_recv()
    total = ws_ref[...]
    for k in range(h - 1):
        total = total + gq[k].astype(jnp.float32)
    ws_ref[...] = total * loss_scale
    last.wait_recv()
    ps_ref[...] = (ps_ref[...] + pq[...].astype(jnp.float32)) * loss_scale
    for copy in g_copies + x_copies + y_copies + p_copies + q_copies + sa_copies + [last]:
        copy.wait_send()


def tail(block_input, out_grad, w_value, w_gate, grad_both, mixer_out, small, loss_scale):
    n, n_tp = lax.axis_size("sp"), lax.axis_size("tp")
    tokens, width = block_input.shape
    chans = mixer_out.shape[1]
    rows, cols, h, chunks = width // n, width // n_tp, n // 2, 4
    step = tokens // chunks
    bf, f32 = jnp.bfloat16, jnp.float32
    anywhere = pl.BlockSpec(memory_space=pl.ANY)
    vmem = pl.BlockSpec(memory_space=pltpu.VMEM)
    dma = pltpu.SemaphoreType.DMA
    V = pltpu.VMEM
    return pl.pallas_call(
        functools.partial(tail_kernel, n, n_tp, loss_scale),
        out_shape=(
            jax.ShapeDtypeStruct((tokens, cols), bf),
            jax.ShapeDtypeStruct((rows, 2 * chans), f32),
            jax.ShapeDtypeStruct((rows, chans), f32),
            jax.ShapeDtypeStruct(small.shape, f32),
        ),
        in_specs=[anywhere] * 4 + [vmem] * 3,
        out_specs=(vmem,) * 4,
        scratch_shapes=[
            V((tokens, width), bf), V((tokens, width), bf), V((width, chans), bf), V((width, chans), bf),
            V((width, 2 * chans), bf), V((h, rows, 2 * chans), bf), V((h - 1, rows, 2 * chans), bf),
            V((h - 1, rows, 2 * chans), bf),
            V((width, chans), bf), V((h - 1, 2 * rows, chans), bf), V((rows, chans), bf), V((rows, chans), bf),
            V((chunks, 2, step, cols), bf), V((chunks, 2, step, cols), bf), V((chunks, step, cols), bf),
            V((chunks, step, cols), bf), V((tokens, cols), f32),
            V(small.shape, f32), V(small.shape, f32), V((h,) + small.shape, f32),
            dma((4,)),
            dma((h,)), dma((h,)), dma((h - 1,)), dma((h - 1,)), dma((h - 1,)), dma((h - 1,)), dma((1,)), dma((1,)),
            dma((chunks,)), dma((chunks,)), dma((chunks,)), dma((chunks,)), dma((1,)), dma((1,)),
            dma((h - 1,)), dma((h - 1,)),
        ],
        compiler_params=pltpu.CompilerParams(
            collective_id=0, has_side_effects=True, vmem_limit_bytes=60 * 1024 * 1024
        ),
    )(block_input, out_grad, w_value, w_gate, grad_both, mixer_out, small)


def shards(block_input, out_grad, w_value, w_gate, conv_taps, norm_gain, norm_shift, w_proj):
    tok_rows = block_input.shape[0]
    kernel_len = conv_taps.shape[0]
    reach_back = kernel_len - 1
    channels_dev = w_value.shape[1]
    loss_scale = 1.0 / math.sqrt(tok_rows * lax.axis_size("sp"))
    value_proj = jnp.dot(block_input, w_value, preferred_element_type=jnp.float32).astype(
        jnp.bfloat16
    )
    gate_proj = jnp.dot(block_input, w_gate, preferred_element_type=jnp.float32).astype(
        jnp.bfloat16
    )
    gate_sigmoid = jax.nn.sigmoid(gate_proj.astype(jnp.float32))
    value_wide = value_proj.astype(jnp.float32)
    gated_input = (value_wide * gate_sigmoid).astype(jnp.bfloat16)
    earlier = from_behind(gated_input[tok_rows - reach_back :], "sp", 1)
    extended = jnp.concatenate([earlier, gated_input], axis=0).astype(jnp.float32)
    filtered = jnp.zeros((tok_rows, channels_dev), jnp.float32)
    for tap_index in range(kernel_len):
        begin = reach_back - tap_index
        filtered = filtered + conv_taps[tap_index] * extended[begin : begin + tok_rows]
    row_sum, row_square = lax.psum(
        (jnp.sum(filtered, axis=1), jnp.sum(filtered * filtered, axis=1)), "tp"
    )
    row_mean = row_sum / CH
    row_var = row_square / CH - row_mean * row_mean
    row_scale = lax.rsqrt(row_var + EPS)
    normed = (filtered - row_mean[:, None]) * row_scale[:, None]
    activated = normed * norm_gain + norm_shift
    act_sigmoid = jax.nn.sigmoid(activated)
    mixer_out = (activated * act_sigmoid).astype(jnp.bfloat16)
    grad_mixed = right_product(out_grad, w_proj)
    grad_act = grad_mixed * act_sigmoid * (1.0 + activated * (1.0 - act_sigmoid))
    grad_normed = grad_act * norm_gain
    back_sum, back_cross = lax.psum(
        (jnp.sum(grad_normed, axis=1), jnp.sum(grad_normed * normed, axis=1)), "tp"
    )
    grad_filtered = row_scale[:, None] * (
        grad_normed - back_sum[:, None] / CH - normed * (back_cross[:, None] / CH)
    )
    gain_part = jnp.sum(grad_act * normed, axis=0)
    shift_part = jnp.sum(grad_act, axis=0)
    padded_grad = jnp.pad(grad_filtered, ((reach_back, reach_back), (0, 0)))
    grad_extended = jnp.zeros((tok_rows + reach_back, channels_dev), jnp.float32)
    taps_rows = []
    for tap_index in range(kernel_len):
        begin = reach_back - tap_index
        grad_extended = (
            grad_extended
            + conv_taps[tap_index] * padded_grad[tap_index : tap_index + tok_rows + reach_back]
        )
        taps_rows.append(jnp.sum(grad_filtered * extended[begin : begin + tok_rows], axis=0))
    taps_part = jnp.stack(taps_rows, axis=0)
    returned = from_behind(grad_extended[:reach_back], "sp", -1)
    grad_glu = jnp.concatenate(
        [grad_extended[reach_back:tok_rows], grad_extended[tok_rows:] + returned], axis=0
    )
    grad_value = (grad_glu * gate_sigmoid).astype(jnp.bfloat16)
    grad_gate = (grad_glu * value_wide * gate_sigmoid * (1.0 - gate_sigmoid)).astype(jnp.bfloat16)
    grad_both = jnp.concatenate([grad_value, grad_gate], axis=1)
    small = jnp.concatenate([taps_part, gain_part[None], shift_part[None]], axis=0)
    small = jnp.pad(small, ((0, -small.shape[0] % 8), (0, 0)))
    input_grad, weight_sum, proj_sum, small_sum = tail(
        block_input, out_grad, w_value, w_gate, grad_both, mixer_out, small, loss_scale
    )
    return (
        input_grad,
        weight_sum[:, :channels_dev],
        weight_sum[:, channels_dev:],
        proj_sum.T,
        small_sum[:kernel_len],
        small_sum[kernel_len],
        small_sum[kernel_len + 1],
    )


def solution(mesh):
    return jax.shard_map(
        shards,
        mesh=mesh,
        in_specs=(
            P("sp", None),
            P("sp", None),
            P(None, "tp"),
            P(None, "tp"),
            P(None, "tp"),
            P("tp"),
            P("tp"),
            P("tp", None),
        ),
        out_specs=(
            P("sp", "tp"),
            P("sp", "tp"),
            P("sp", "tp"),
            P("tp", "sp"),
            P(None, "tp"),
            P("tp"),
            P("tp"),
        ),
        check_vma=False,
    )
```

profile of v0, /device:TPU:9, one launch (start us, length us, event | category | flops | bytes accessed | tf_op | source)
XLA Modules:
  0.0 122.0 jit_solution(15503223437446943897)
XLA Ops:
  0.7 3.9 %convolution_convert_fusion.1 = bf16[1024,256]{1,0:T(8,128)(2,1)S(1)} fusion(bf16[1024,2048]{1,0:T(8,128)(2,1)} %bi_hbm.1, bf16[2048,256]{1,0:T(8,128)(2,1)} %wv_hbm.1), kind=kOutput, calls=%fused_computation.10 | convolution fusion | flops 1074003968 | bytes 5767168 | tf_op jit(solution)/shard_map/dot_general | solution.py:261
  4.6 0.2 copy-done.2
  4.8 2.3 %fusion.6 = (bf16[1024,256]{1,0:T(8,128)(2,1)S(1)}, f32[1024,256]{1,0:T(8,128)}) fusion(bf16[1024,256]{1,0:T(8,128)(2,1)S(1)} %convolution_convert_fusion.1, bf16[1024,2048]{1,0:T(8,128)(2,1)S(1)} %copy-done.1, bf16[2048,256]{1,0:T(8,128)(2,1)S(1)} %copy-done.2), kind=kOutput, calls=%fused_computation.12 | convolution fusion | flops 1075838976 | bytes 7340032 | tf_op jit(solution)/shard_map/dot_general | solution.py:264
  7.1 3.1 %collective-permute-start = (bf16[30,256]{1,0:T(8,128)(2,1)S(1)}, bf16[30,256]{1,0:T(8,128)(2,1)S(1)}, u32[]{:S(2)}, u32[]{:S(2)}) collective-permute-start(bf16[30,256]{1,0:T(8,128)(2,1)S(1)} %slice.470), channel_id=1, source_target_pairs={{0,4},{4,8},{8,12},{12,16},{16,20},{20,24},{24,28},{1,5},{5,9},{9,... | collective-permute-start | bytes 46088 | tf_op jit(solution)/shard_map/ppermute | solution.py:20
  10.3 2.2 %collective-permute-done = bf16[30,256]{1,0:T(8,128)(2,1)S(1)} collective-permute-done((bf16[30,256]{1,0:T(8,128)(2,1)S(1)}, bf16[30,256]{1,0:T(8,128)(2,1)S(1)}, u32[]{:S(2)}, u32[]{:S(2)}) %collective-permute-start) | collective-permute-done | bytes 15392 | tf_op jit(solution)/shard_map/ppermute | solution.py:20
  12.5 0.1 maximum_convert_fusion
  12.6 4.6 %multiply_reduce_fusion.33 = (f32[1024]{0:T(1024)S(1)}, f32[1024]{0:T(1024)S(1)}, f32[1024,256]{1,0:T(8,128)S(1)}) fusion(f32[1054,256]{1,0:T(8,128)S(1)} %maximum_convert_fusion, f32[256]{0:T(256)S(1)} %bitcast.132, f32[256]{0:T(256)S(1)} %bitcast.134, f32[256]{0:T(256)S(1)} %bitcast.76, f32[256]{0:T(256)S(1)} %bitcast.78, f32[256]{0:T(256)S(1)} %bitcast.80, ...), kind=kLoop, calls=%fused_computation.57 | loop fusion | flops 16775168 | bytes 33594368 | tf_op jit(solution)/shard_map/reduce_sum | solution.py:277
  17.2 6.9 %all-reduce.3 = (f32[1024]{0:T(1024)S(1)}, f32[1024]{0:T(1024)S(1)}) all-reduce(f32[1024]{0:T(1024)S(1)} %get-tuple-element.58, f32[1024]{0:T(1024)S(1)} %get-tuple-element.57), channel_id=1, replica_groups=mesh['sp'=8,'tp'=4] {'tp'}, use_global_device_ids=true, to_apply=%region_3.0 | all-reduce | flops 2048 | bytes 16384 | tf_op jit(solution)/shard_map/psum | solution.py:276
  24.2 4.8 %multiply_reduce_fusion = (f32[256]{0:T(256)S(1)}, f32[1024]{0:T(1024)S(1)}, f32[1024]{0:T(1024)S(1)}, f32[256]{0:T(256)S(1)}, bf16[1024,256]{1,0:T(8,128)(2,1)}, /*index=5*/f32[1024,256]{1,0:T(8,128)}) fusion(f32[1024,256]{1,0:T(8,128)S(1)} %get-tuple-element.64, f32[1024]{0:T(1024)S(1)} %get-tuple-element.104, f32[1024]{0:T(1024)S(1)} %get-tuple-element.103, ...), kind=kOutput, calls=%fused_computation.18 | convolution fusion | flops 1079244288 | bytes 7884800 | tf_op jit(solution)/shard_map/dot_general | solution.py:24
  29.1 5.9 %all-reduce.2 = (f32[1024]{0:T(1024)S(1)}, f32[1024]{0:T(1024)S(1)}) all-reduce(f32[1024]{0:T(1024)S(1)} %get-tuple-element.54, f32[1024]{0:T(1024)S(1)} %get-tuple-element.55), channel_id=1, replica_groups=mesh['sp'=8,'tp'=4] {'tp'}, use_global_device_ids=true, to_apply=%region_7.0 | all-reduce | flops 2048 | bytes 16384 | tf_op jit(solution)/shard_map/psum | solution.py:289
  34.9 4.3 %multiply_reduce_fusion.1 = (f32[256]{0:T(256)S(1)}, f32[256]{0:T(256)S(1)}, f32[256]{0:T(256)S(1)}, f32[256]{0:T(256)S(1)}, f32[256]{0:T(256)S(1)}, /*index=5*/...) fusion(f32[1054,256]{1,0:T(8,128)S(1)} %maximum_convert_fusion,, ...), kind=kLoop, calls=%fused_computation.19 | loop fusion | flops 11267584 | bytes 22055936 | tf_op jit(solution)/shard_map/reduce_sum | solution.py:306
  39.2 4.9 %multiply_add_fusion = f32[1054,256]{1,0:T(8,128)S(1)} fusion(f32[1024,256]{1,0:T(8,128)S(1)} %get-tuple-element.63, f32[256]{0:T(256)S(1)} %bitcast.133, f32[256]{0:T(256)S(1)} %bitcast.135, f32[256]{0:T(256)S(1)} %bitcast.77, f32[256]{0:T(256)S(1)} %bitcast.79, f32[256]{0:T(256)S(1)} %bitcast.81, f32[256]{0:T(256)S(1)} %bitcast.83, f32[256]{0:T(256)S(1)} %bitcast.85, ...), kind=kLoop, calls=%fused_computation.11 | loop fusion | flops 16459264 | bytes 2159616 | tf_op jit(solution)/shard_map/add | solution.py:303
  44.2 2.3 %collective-permute-start.1 = (f32[30,256]{1,0:T(8,128)S(1)}, f32[30,256]{1,0:T(8,128)S(1)}, u32[]{:S(2)}, u32[]{:S(2)}) collective-permute-start(f32[30,256]{1,0:T(8,128)S(1)} %slice.504), channel_id=1, source_target_pairs={{4,0},{8,4},{12,8},{16,12},{20,16},{24,20},{28,24},{5,1},{9,5},{13... | collective-permute-start | bytes 92168 | tf_op jit(solution)/shard_map/ppermute | solution.py:20
  46.5 1.8 %multiply_reduce_fusion.19 = (f32[256]{0:T(256)S(1)}, f32[256]{0:T(256)S(1)}, f32[256]{0:T(256)S(1)}, f32[256]{0:T(256)S(1)}, f32[256]{0:T(256)S(1)}, /*index=5*...) fusion(f32[1024,256]{1,0:T(8,128)S(1)} %get-tuple-element.63, ...), kind=kLoop, calls=%fused_computation.37 | loop fusion | flops 6812416 | bytes 14693376 | tf_op jit(solution)/shard_map/reduce_sum | solution.py:306
  48.3 0.1 concatenate.15
  48.4 0.6 pad.9.small_ref
  49.1 1.6 %multiply_convert_fusion.1 = (bf16[1024,256]{1,0:T(8,128)(2,1)S(1)}, bf16[1024,256]{1,0:T(8,128)(2,1)S(1)}) fusion(f32[1024,256]{1,0:T(8,128)} %get-tuple-element.106, f32[30,256]{1,0:T(8,128)S(1)} %slice_add_fusion, f32[994,256]{1,0:T(8,128)S(1)} %slice.502, bf16[1024,256]{1,0:T(8,128)(2,1)} %copy-done.4), kind=kLoop, calls=%fused_computation.51 | loop fusion | flops 2359296 | bytes 3670016 | tf_op jit(solution)/shard_map/convert_element_type | solution.py:312
  50.7 1.1 pad_maximum_fusion.1.gb_ref
  51.8 62.9 %shard_map.135 = (bf16[1024,512]{1,0:T(8,128)(2,1)}, f32[256,512]{1,0:T(8,128)}, f32[256,256]{1,0:T(8,128)}, f32[40,256]{1,0:T(8,128)}) custom-call(bf16[1024,2048]{1,0:T(8,128)(2,1)} %bi_hbm.1, bf16[1024,2048]{1,0:T(8,128)(2,1)} %og_hbm.1, bf16[2048,256]{1,0:T(8,128)(2,1)} %wv_hbm.1, bf16[2048,256]{1,0:T(8,128)(2,1)} %wg_hbm.1, ...), custom_call_target="tpu_custom_call" | custom-call | tf_op jit(solution)/shard_map/pallas_call | solution.py:226
  114.7 1.4 %fusion.11 = (f32[1,256]{1,0:T(1,128)}, f32[1,256]{1,0:T(1,128)}) fusion(f32[40,256]{1,0:T(8,128)} %get-tuple-element.14), kind=kLoop, calls=%fused_computation.67 | loop fusion | bytes 4096 | tf_op jit(solution)/shard_map/slice | solution.py:327
  116.0 1.4 %slice.467 = f32[31,256]{1,0:T(8,128)} slice(f32[40,256]{1,0:T(8,128)} %get-tuple-element.14), slice={[0:31], [0:256]} | slice | bytes 63488 | tf_op jit(solution)/shard_map/slice | solution.py:325
  117.4 1.8 %copy.15 = f32[256,256]{1,0:T(8,128)} copy(f32[256,256]{0,1:T(8,128)} %bitcast.73) | data formatting | bytes 524288
  119.2 1.9 %fusion.10 = (f32[256,256]{1,0:T(8,128)}, f32[256,256]{1,0:T(8,128)}) fusion(f32[256,512]{1,0:T(8,128)} %get-tuple-element.12), kind=kLoop, calls=%fused_computation.66 | loop fusion | bytes 1048576 | tf_op jit(solution)/shard_map/slice | solution.py:323
  121.1 1.0 copy.17
  (24 shorter events, 0.2 us)
Async XLA Ops:
  0.6 23.6 %copy-start = (bf16[256,2048]{1,0:T(8,128)(2,1)S(1)}, bf16[256,2048]{1,0:T(8,128)(2,1)}, u32[]{:S(2)}) copy-start(bf16[256,2048]{1,0:T(8,128)(2,1)} %param.15) | copy-start | bytes 3145732
  0.6 3.9 %copy-start.1 = (bf16[1024,2048]{1,0:T(8,128)(2,1)S(1)}, bf16[1024,2048]{1,0:T(8,128)(2,1)}, u32[]{:S(2)}) copy-start(bf16[1024,2048]{1,0:T(8,128)(2,1)} %bi_hbm.1) | copy-start | bytes 12582916
  0.7 4.1 %copy-start.2 = (bf16[2048,256]{1,0:T(8,128)(2,1)S(1)}, bf16[2048,256]{1,0:T(8,128)(2,1)}, u32[]{:S(2)}) copy-start(bf16[2048,256]{1,0:T(8,128)(2,1)} %wg_hbm.1) | copy-start | bytes 3145732
  4.8 2.3 %copy-start.4 = (bf16[1024,256]{1,0:T(8,128)(2,1)}, bf16[1024,256]{1,0:T(8,128)(2,1)S(1)}, u32[]{:S(2)}) copy-start(bf16[1024,256]{1,0:T(8,128)(2,1)S(1)} %convolution_convert_fusion.1) | copy-start | bytes 1572868
  4.8 5.4 %copy-start.5 = (f32[31,256]{1,0:T(8,128)S(1)}, f32[31,256]{1,0:T(8,128)}, u32[]{:S(2)}) copy-start(f32[31,256]{1,0:T(8,128)} %param.12) | copy-start | bytes 95236
  7.1 5.4 %collective-permute-start = (bf16[30,256]{1,0:T(8,128)(2,1)S(1)}, bf16[30,256]{1,0:T(8,128)(2,1)S(1)}, u32[]{:S(2)}, u32[]{:S(2)}) collective-permute-start(bf16[30,256]{1,0:T(8,128)(2,1)S(1)} %slice.470), channel_id=1, source_target_pairs={{0,4},{4,8},{8,12},{12,16},{16,20},{20,24},{24,28},{1,5},{5,9},{9,... | collective-permute-start | bytes 46088 | tf_op jit(solution)/shard_map/ppermute | solution.py:20
  12.6 11.6 %copy-start.6 = (f32[256]{0:T(256)S(1)}, f32[256]{0:T(256)}, u32[]{:S(2)}) copy-start(f32[256]{0:T(256)} %param.13) | copy-start | bytes 3076
  12.6 11.6 %copy-start.7 = (f32[256]{0:T(256)S(1)}, f32[256]{0:T(256)}, u32[]{:S(2)}) copy-start(f32[256]{0:T(256)} %param.14) | copy-start | bytes 3076
  44.2 4.9 %collective-permute-start.1 = (f32[30,256]{1,0:T(8,128)S(1)}, f32[30,256]{1,0:T(8,128)S(1)}, u32[]{:S(2)}, u32[]{:S(2)}) collective-permute-start(f32[30,256]{1,0:T(8,128)S(1)} %slice.504), channel_id=1, source_target_pairs={{4,0},{8,4},{12,8},{16,12},{20,16},{24,20},{28,24},{5,1},{9,5},{13... | collective-permute-start | bytes 92168 | tf_op jit(solution)/shard_map/ppermute | solution.py:20
  114.7 6.4 %copy-start.3 = (bf16[1024,512]{1,0:T(8,128)(2,1)S(1)}, bf16[1024,512]{1,0:T(8,128)(2,1)}, u32[]{:S(2)}) copy-start(bf16[1024,512]{1,0:T(8,128)(2,1)} %get-tuple-element.117) | copy-start | bytes 3145732
where the time goes:
time: 122 us
  Pallas kernels  62.9 us (52%)
  other arithmetic  18.4 us (15%)
  blocking collectives  12.8 us (10%)
  matrix products  11 us (9%)
  local copies, waits for them, and re-layouts  8.47 us (7%)
  starting transfers between devices  5.47 us (4%)
  waiting for transfers between devices  2.17 us (2%)
    pallas_call x1, Pallas kernels, tail(): pl.pallas_call(functools.partial(tail_kernel, n, n_tp, loss_scale), out_s...  62.9 us
    psum x1, blocking collectives, shards(): lax.psum((jnp.sum(filtered, axis=1), jnp.sum(filtered * filtered, axis=1)...  6.92 us
    reduce_sum x2, other arithmetic, shards(): jnp.sum(grad_filtered * extended[begin:begin + tok_rows], axis=0)  6.07 us
    psum x1, blocking collectives, shards(): lax.psum((jnp.sum(grad_normed, axis=1), jnp.sum(grad_normed * normed, axi...  5.85 us
    ppermute x2, starting transfers between devices, from_behind(): return lax.ppermute(block, axis, route)  5.47 us
    add x1, other arithmetic, shards(): grad_extended + conv_taps[tap_index] * padded_grad[tap_index:tap_index +...  4.89 us
    dot_general x1, matrix products, right_product(): lax.dot_general(left, right, (((1,), (1,)), ((), ())), preferred_element_...  4.83 us
    reduce_sum x1, other arithmetic, shards(): jnp.sum(filtered * filtered, axis=1)  4.65 us
  transfers between devices with their start and end apart: 2, of which 1 were waited for; matrix products, arithmetic and copies ran while one was open for 2% of the time, Pallas kernels for 0%

commit v1 on v0

v1 whole, which is shorter than its diff:
```python
import functools
import math

import jax
import jax.numpy as jnp
from jax import lax
from jax.experimental import pallas as pl
from jax.experimental.pallas import tpu as pltpu
from jax.sharding import PartitionSpec as P

EPS = 0.05
MESH = pl.DeviceIdType.MESH
LANES = 128
BF, F32 = jnp.bfloat16, jnp.float32


def right_product(left, right):
    return lax.dot_general(
        left, right, (((1,), (1,)), ((), ())), preferred_element_type=F32
    )


def column_product(left, right):
    return lax.dot_general(
        left, right, (((0,), (0,)), ((), ())), preferred_element_type=F32
    )


def main_kernel(
    n, n_tp, n_chan, halo,
    bi_hbm, og_hbm, wv_hbm, wg_hbm, wp_hbm, taps_ref, gain_ref, shift_ref,
    ig_ref, ws_ref, ps_ref, sm_ref,
    bi, og, wv, wg, wp,
    gx, vp, sg, fl, nm, gn, gf, gm, mo, gb, tacc, cols, rowbuf, so, si,
    gs, gr, gs2, gq, pm, pr, pm2, pq,
    xs, xr, ys, yr, acc, small, small_pair, small_in, small_all,
    load_sem, st_send, st_recv, hx_send, hx_recv, hf_send, hf_recv,
    gs_send, gs_recv, gq_send, gq_recv, pr_send, pr_recv, pq_send, pq_recv,
    x_send, x_recv, y_send, y_recv, s_send, s_recv, sa_send, sa_recv,
):
    me, t = lax.axis_index("sp"), lax.axis_index("tp")
    outer, inner = me // 2, me % 2
    h = n // 2
    mate = 2 * outer + (1 - inner)
    t_near, t_far = t + 1 - 2 * (t % 2), lax.rem(t + n_tp // 2, n_tp)
    t_cross = lax.rem(t_near + n_tp // 2, n_tp)
    tokens, width = bi.shape
    rows, cols_tp = width // n, width // n_tp
    chans = wv.shape[1]
    halves = chans // LANES
    kernel_len = taps_ref.shape[0]
    chunks = xs.shape[0]
    step = tokens // chunks
    block = 64
    per = step // block

    def load(src, dst, i):
        copy = pltpu.make_async_copy(src, dst, load_sem.at[i])
        copy.start()
        return copy

    def piece(r):
        return pl.ds(r * step, step)

    order_in = [chunks - 1] + list(range(chunks - 1))
    load_w = [load(wv_hbm, wv, 0), load(wg_hbm, wg, 1)]
    load_bi = {r: load(bi_hbm.at[piece(r)], bi.at[piece(r)], 3 + r) for r in order_in}
    load_wp = load(wp_hbm, wp, 2)
    load_og = [load(og_hbm.at[piece(r)], og.at[piece(r)], 3 + chunks + r) for r in range(chunks)]

    barrier = pltpu.get_barrier_semaphore()
    peers = [{"sp": 2 * lax.rem(outer + k, h) + inner} for k in range(1, h)]
    peers += [{"sp": mate}, {"sp": lax.rem(me + 1, n)}, {"sp": lax.rem(me + n - 1, n)}]
    peers += [{"tp": lax.rem(t + k, n_tp)} for k in range(1, n_tp)]
    for who in peers:
        pl.semaphore_signal(barrier, inc=1, device_id=who, device_id_type=MESH)

    first, last = me == 0, me == n - 1
    tacc[...] = jnp.zeros_like(tacc)

    @pl.when(first)
    def _():
        gx[:, :halo, :] = jnp.zeros((halves, halo, LANES), F32)

    @pl.when(last)
    def _():
        gf[:, tokens:, :] = jnp.zeros((halves, halo, LANES), F32)

    pl.semaphore_wait(barrier, len(peers))

    def describe(src, dst, send_sem, recv_sem, who):
        return pltpu.make_async_remote_copy(
            src_ref=src, dst_ref=dst, send_sem=send_sem, recv_sem=recv_sem,
            device_id=who, device_id_type=MESH,
        )

    def send(*args):
        copy = describe(*args)
        copy.start()
        return copy

    sent = []

    halo_x = describe(
        gx.at[:, pl.ds(tokens, halo), :], gx.at[:, pl.ds(0, halo), :],
        hx_send.at[0], hx_recv.at[0], {"sp": lax.rem(me + 1, n)},
    )
    for copy in load_w:
        copy.wait()
    for r in order_in:
        load_bi[r].wait()
        where = piece(r)
        value = jnp.dot(bi[where, :], wv[...], preferred_element_type=F32).astype(BF)
        gate = jnp.dot(bi[where, :], wg[...], preferred_element_type=F32).astype(BF).astype(F32)
        sigmoid = jax.nn.sigmoid(gate)
        gated = (value.astype(F32) * sigmoid).astype(BF).astype(F32)
        vp[where, :] = value
        sg[where, :] = sigmoid
        for c in range(halves):
            gx[c, pl.ds(halo + r * step, step), :] = gated[:, c * LANES:(c + 1) * LANES]
        if r == chunks - 1:
            @pl.when(me < n - 1)
            def _():
                halo_x.start()

    @pl.when(me > 0)
    def _():
        halo_x.wait_recv()

    lane = lax.broadcasted_iota(jnp.int32, (block, LANES), 1)

    def send_stats(phase, r):
        so[phase, r] = rowbuf[...].T[:8]
        copies = [
            send(so.at[phase, r], si.at[phase, r, k - 1], st_send.at[phase, r, k - 1],
                 st_recv.at[phase, r, k - 1], {"tp": lax.rem(t + k, n_tp)})
            for k in range(1, n_tp)
        ]
        sent.extend(copies)
        return copies

    def take_stats(phase, r, copies):
        total = so[phase, r]
        for k, copy in enumerate(copies):
            copy.wait_recv()
            total = total + si[phase, r, k]
        return total / n_chan

    def rows_of(base, i):
        return pl.ds(pl.multiple_of(base + i * block, block), block)

    def pair_of_sums(i, first_sum, second_sum):
        rowbuf[rows_of(0, i), :] = jnp.where(
            lane == 0, first_sum, jnp.where(lane == 1, second_sum, 0.0)
        )

    def conv_chunk(r):
        def body(i, carry):
            sums = jnp.zeros((block, LANES), F32)
            squares = jnp.zeros((block, LANES), F32)
            for c in range(halves):
                total = jnp.zeros((block, LANES), F32)
                for k in range(kernel_len):
                    where = pl.ds(r * step + i * block + halo - k, block)
                    total = total + taps_ref[pl.ds(k, 1), c * LANES:(c + 1) * LANES] * gx[c, where, :]
                fl[c, rows_of(r * step, i), :] = total
                sums = sums + total
                squares = squares + total * total
            pair_of_sums(i, jnp.sum(sums, axis=1, keepdims=True), jnp.sum(squares, axis=1, keepdims=True))
            return carry

        lax.fori_loop(0, per, body, 0)
        return send_stats(0, r)

    moments = [conv_chunk(r) for r in range(chunks)]

    load_wp.wait()

    def norm_chunk(r, carry):
        load_og[r].wait()
        gm[...] = right_product(og[piece(r), :], wp[...])
        total = take_stats(0, r, moments[r])
        mean = total[0:1]
        scale = lax.rsqrt(total[1:2] - mean * mean + EPS)
        both = jnp.where(lax.broadcasted_iota(jnp.int32, total.shape, 0) == 0, mean, scale)
        cols[0, piece(r), :8] = both.T

        def body(i, carry):
            where = rows_of(r * step, i)
            mean = cols[0, where, 0:1]
            scale = cols[0, where, 1:2]
            sums = jnp.zeros((block, LANES), F32)
            crosses = jnp.zeros((block, LANES), F32)
            out = []
            for c in range(halves):
                at = slice(c * LANES, (c + 1) * LANES)
                gain, shift = gain_ref[:, at], shift_ref[:, at]
                normed = (fl[c, where, :] - mean) * scale
                activated = normed * gain + shift
                sigmoid = jax.nn.sigmoid(activated)
                mo[where, at] = (activated * sigmoid).astype(BF)
                grad_act = gm[rows_of(0, i), at] * sigmoid * (1.0 + activated * (1.0 - sigmoid))
                grad_normed = grad_act * gain
                nm[c, where, :] = normed
                gn[c, where, :] = grad_normed
                sums = sums + grad_normed
                crosses = crosses + grad_normed * normed
                fold = lambda x: x.reshape(block // 8, 8, LANES).sum(axis=0)
                out.append(carry[2 * c] + fold(grad_act * normed))
                out.append(carry[2 * c + 1] + fold(grad_act))
            pair_of_sums(i, jnp.sum(sums, axis=1, keepdims=True), jnp.sum(crosses, axis=1, keepdims=True))
            return tuple(out)

        carry = lax.fori_loop(0, per, body, carry)
        return send_stats(1, r), carry

    carry = tuple(jnp.zeros((8, LANES), F32) for _ in range(2 * halves))
    means = []
    for r in range(chunks):
        copies, carry = norm_chunk(r, carry)
        means.append(copies)
    small[...] = jnp.zeros_like(small)
    for c in range(halves):
        at = slice(c * LANES, (c + 1) * LANES)
        small[kernel_len:kernel_len + 1, at] = carry[2 * c].sum(axis=0, keepdims=True)
        small[kernel_len + 1:kernel_len + 2, at] = carry[2 * c + 1].sum(axis=0, keepdims=True)

    aligned = rows % LANES == 0
    wide = 256
    order = [lax.rem(outer + k, h) for k in range(1, h)] + [outer]

    def block_rows(o, i):
        return pl.ds(pl.multiple_of((2 * o + i) * rows, rows), rows)

    def make_block(store, act, other, o, i):
        if aligned:
            where = block_rows(o, i)
            store[where, :] = column_product(act[:, where], other[...]).astype(BF)

    def make_all(store, act, other):
        if not aligned:
            for c in range(width // wide):
                where = pl.ds(c * wide, wide)
                store[where, :] = column_product(act[:, where], other[...]).astype(BF)

    def mate_block(store, act, other, landing, send_sem, recv_sem, k):
        make_block(store, act, other, order[k], 1 - inner)
        where = block_rows(order[k], 1 - inner)
        return send(store.at[where], landing.at[k], send_sem.at[k], recv_sem.at[k], {"sp": mate})

    def outer_block(store, act, other, landing, copies, second, landed, send_sem, recv_sem, k):
        make_block(store, act, other, order[k], inner)
        copies[k].wait_recv()
        total = store[block_rows(order[k], inner), :].astype(F32) + landing[k].astype(F32)
        if k == h - 1:
            return total
        second[k] = total.astype(BF)
        return send(second.at[k], landed.at[k], send_sem.at[k], recv_sem.at[k], {"sp": 2 * order[k] + inner})

    make_all(pm, og, mo)
    p_copies = [mate_block(pm, og, mo, pr, pr_send, pr_recv, k) for k in range(h)]
    p_outer = []

    def proj_outer(k):
        p_outer.append(outer_block(pm, og, mo, pr, p_copies, pm2, pq, pq_send, pq_recv, k))

    halo_f = describe(
        gf.at[:, pl.ds(0, halo), :], gf.at[:, pl.ds(tokens, halo), :],
        hf_send.at[0], hf_recv.at[0], {"sp": lax.rem(me + n - 1, n)},
    )

    def filtered_chunk(r):
        cols[1, piece(r), :8] = take_stats(1, r, means[r]).T

        def body(i, carry):
            where = rows_of(r * step, i)
            scale = cols[0, where, 1:2]
            first_mean = cols[1, where, 0:1]
            second_mean = cols[1, where, 1:2]
            for c in range(halves):
                gf[c, where, :] = scale * (
                    gn[c, where, :] - first_mean - nm[c, where, :] * second_mean
                )
            return carry

        lax.fori_loop(0, per, body, 0)

    def back_chunk(r):
        def body(i, carry):
            where = rows_of(r * step, i)
            for c in range(halves):
                at = slice(c * LANES, (c + 1) * LANES)
                gated = gx[c, pl.ds(pl.multiple_of(r * step + i * block + halo, 32), block), :]
                total = jnp.zeros((block, LANES), F32)
                for k in range(kernel_len):
                    grad = gf[c, pl.ds(r * step + i * block + k, block), :]
                    total = total + taps_ref[pl.ds(k, 1), at] * grad
                    tacc[c, k] += (gated * grad).reshape(block // 8, 8, LANES).sum(axis=0)
                sigmoid = sg[where, at]
                value = vp[where, at].astype(F32)
                gb[where, at] = (total * sigmoid).astype(BF)
                gb[where, chans + c * LANES:chans + (c + 1) * LANES] = (
                    total * value * sigmoid * (1.0 - sigmoid)
                ).astype(BF)
            return carry

        lax.fori_loop(0, per, body, 0)

    def partial_input(r, j):
        at = pl.ds(pl.multiple_of(j * cols_tp, cols_tp), cols_tp)
        return right_product(gb[piece(r), :chans], wv[at, :]) + right_product(
            gb[piece(r), chans:], wg[at, :]
        )

    x_copies, y_copies = [], []

    def near_block(r):
        xs[r, 0] = partial_input(r, t_cross).astype(BF)
        xs[r, 1] = partial_input(r, t_near).astype(BF)
        x_copies.append(send(xs.at[r], xr.at[r], x_send.at[r], x_recv.at[r], {"tp": t_near}))

    def far_block(r):
        far = partial_input(r, t_far)
        x_copies[r].wait_recv()
        ys[r] = (far + xr[r, 0].astype(F32)).astype(BF)
        y_copies.append(send(ys.at[r], yr.at[r], y_send.at[r], y_recv.at[r], {"tp": t_far}))
        acc[piece(r), :] = partial_input(r, t) + xr[r, 1].astype(F32)

    filtered_chunk(0)

    @pl.when(me > 0)
    def _():
        halo_f.start()

    stage = 0
    for r in range(chunks):
        if r + 1 < chunks:
            filtered_chunk(r + 1)
        else:
            @pl.when(me < n - 1)
            def _():
                halo_f.wait_recv()
        back_chunk(r)
        near_block(r)
        while stage < h * (r + 1) // chunks:
            proj_outer(stage)
            stage += 1
        if r:
            far_block(r - 1)

    make_all(gs, bi, gb)
    g_copies = [mate_block(gs, bi, gb, gr, gs_send, gs_recv, k) for k in range(h)]
    far_block(chunks - 1)

    for c in range(halves):
        small[:kernel_len, c * LANES:(c + 1) * LANES] = tacc[c].sum(axis=1)
    small_copy = send(small, small_in, s_send.at[0], s_recv.at[0], {"sp": mate})
    g_outer = []
    for k in range(h):
        g_outer.append(outer_block(gs, bi, gb, gr, g_copies, gs2, gq, gq_send, gq_recv, k))
        if k == 0:
            small_copy.wait_recv()
            small_pair[...] = small[...] + small_in[...]
            sa_copies = [
                send(small_pair, small_all.at[outer], sa_send.at[j - 1], sa_recv.at[j - 1],
                     {"sp": 2 * lax.rem(outer + j, h) + inner})
                for j in range(1, h)
            ]

    loss_scale = 1.0 / math.sqrt(tokens * n)
    total = p_outer.pop()
    for k, copy in enumerate(p_outer):
        copy.wait_recv()
        total = total + pq[k].astype(F32)
    ps_ref[...] = total * loss_scale
    for copy in sa_copies:
        copy.wait_recv()
    small_all[outer] = small_pair[...]
    total = small_all[0]
    for k in range(1, h):
        total = total + small_all[k]
    sm_ref[...] = total * loss_scale
    for r in range(chunks):
        y_copies[r].wait_recv()
        ig_ref[piece(r), :] = (acc[piece(r), :] + yr[r].astype(F32)).astype(BF)
    total = g_outer.pop()
    for k, copy in enumerate(g_outer):
        copy.wait_recv()
        total = total + gq[k].astype(F32)
    ws_ref[...] = total * loss_scale

    @pl.when(me < n - 1)
    def _():
        halo_x.wait_send()

    @pl.when(me > 0)
    def _():
        halo_f.wait_send()

    for copy in sent + p_copies + p_outer + x_copies + y_copies + g_copies + g_outer + sa_copies + [small_copy]:
        copy.wait_send()


def finish_kernel(
    ig_ref, ws_ref, ps_ref, sm_ref, ig_out, wv_out, wg_out, wp_out, taps_out, gain_out, shift_out,
    turned, taps, gain, shift, sems,
):
    chans = ps_ref.shape[1]
    kernel_len = taps_out.shape[0]
    copies = []

    def store(src, dst):
        copies.append(pltpu.make_async_copy(src, dst, sems.at[len(copies)]))
        copies[-1].start()

    store(ig_ref, ig_out)
    store(ws_ref.at[:, :chans], wv_out)
    store(ws_ref.at[:, chans:], wg_out)
    taps[...] = sm_ref[:kernel_len]
    gain[...] = sm_ref[kernel_len:kernel_len + 1]
    shift[...] = sm_ref[kernel_len + 1:kernel_len + 2]
    store(taps, taps_out)
    store(gain, gain_out)
    store(shift, shift_out)
    turned[...] = ps_ref[...].T
    store(turned, wp_out)
    for copy in copies:
        copy.wait()


def shards(block_input, out_grad, w_value, w_gate, conv_taps, norm_gain, norm_shift, w_proj):
    n, n_tp = lax.axis_size("sp"), lax.axis_size("tp")
    tokens, width = block_input.shape
    chans = w_value.shape[1]
    kernel_len = conv_taps.shape[0]
    halves = chans // LANES
    halo = -(-(kernel_len - 1) // 8) * 8
    rows, cols, h, chunks = width // n, width // n_tp, n // 2, 4
    step = tokens // chunks
    smalls = (-(-(kernel_len + 2) // 8) * 8, chans)
    anywhere = pl.BlockSpec(memory_space=pl.ANY)
    vmem = pl.BlockSpec(memory_space=pltpu.VMEM)
    dma = pltpu.SemaphoreType.DMA
    V = pltpu.VMEM
    shape = jax.ShapeDtypeStruct
    results = pl.pallas_call(
        functools.partial(main_kernel, n, n_tp, chans * n_tp, halo),
        out_shape=(
            shape((tokens, cols), BF), shape((rows, 2 * chans), F32),
            shape((rows, chans), F32), shape(smalls, F32),
        ),
        in_specs=[anywhere] * 5 + [vmem] * 3,
        out_specs=(vmem,) * 4,
        scratch_shapes=[
            V((tokens, width), BF), V((tokens, width), BF), V((width, chans), BF), V((width, chans), BF),
            V((chans, width), BF),
            V((halves, halo + tokens, LANES), F32), V((tokens, chans), BF), V((tokens, chans), F32),
            V((halves, tokens, LANES), F32), V((halves, tokens, LANES), F32), V((halves, tokens, LANES), F32),
            V((halves, tokens + halo, LANES), F32), V((step, chans), F32), V((tokens, chans), BF),
            V((tokens, 2 * chans), BF), V((halves, kernel_len, 8, LANES), F32), V((2, tokens, LANES), F32),
            V((step, LANES), F32), V((2, chunks, 8, step), F32), V((2, chunks, n_tp - 1, 8, step), F32),
            V((width, 2 * chans), BF), V((h, rows, 2 * chans), BF), V((h - 1, rows, 2 * chans), BF),
            V((h - 1, rows, 2 * chans), BF),
            V((width, chans), BF), V((h, rows, chans), BF), V((h - 1, rows, chans), BF),
            V((h - 1, rows, chans), BF),
            V((chunks, 2, step, cols), BF), V((chunks, 2, step, cols), BF), V((chunks, step, cols), BF),
            V((chunks, step, cols), BF), V((tokens, cols), F32),
            V(smalls, F32), V(smalls, F32), V(smalls, F32), V((h,) + smalls, F32),
            dma((3 + 2 * chunks,)), dma((2, chunks, n_tp - 1)), dma((2, chunks, n_tp - 1)),
            dma((1,)), dma((1,)), dma((1,)), dma((1,)),
            dma((h,)), dma((h,)), dma((h - 1,)), dma((h - 1,)), dma((h,)), dma((h,)), dma((h - 1,)), dma((h - 1,)),
            dma((chunks,)), dma((chunks,)), dma((chunks,)), dma((chunks,)), dma((1,)), dma((1,)),
            dma((h - 1,)), dma((h - 1,)),
        ],
        compiler_params=pltpu.CompilerParams(
            collective_id=0, has_side_effects=True, vmem_limit_bytes=56 * 1024 * 1024
        ),
        name="main",
    )(
        block_input, out_grad, w_value, w_gate, w_proj, conv_taps,
        norm_gain.reshape(1, chans), norm_shift.reshape(1, chans),
    )
    outs = pl.pallas_call(
        finish_kernel,
        out_shape=(
            shape((tokens, cols), BF), shape((rows, chans), F32), shape((rows, chans), F32),
            shape((chans, rows), F32), shape((kernel_len, chans), F32), shape((1, chans), F32), shape((1, chans), F32),
        ),
        in_specs=[vmem] * 4,
        out_specs=(anywhere,) * 7,
        scratch_shapes=[
            V((chans, rows), F32), V((kernel_len, chans), F32), V((1, chans), F32), V((1, chans), F32), dma((7,)),
        ],
        name="finish",
    )(*results)
    return outs[:5] + (outs[5].reshape(chans), outs[6].reshape(chans))


def solution(mesh):
    return jax.shard_map(
        shards,
        mesh=mesh,
        in_specs=(
            P("sp", None),
            P("sp", None),
            P(None, "tp"),
            P(None, "tp"),
            P(None, "tp"),
            P("tp"),
            P("tp"),
            P("tp", None),
        ),
        out_specs=(
            P("sp", "tp"),
            P("sp", "tp"),
            P("sp", "tp"),
            P("tp", "sp"),
            P(None, "tp"),
            P("tp"),
            P("tp"),
        ),
        check_vma=False,
    )
```

time: 122 us -> 86.1 us (0.71)
  the two profiles are of different devices: /device:TPU:9 before, /device:TPU:14 now
where the time goes in v1:
time: 86.1 us; the launch traced here: 85.9 us
  Pallas kernels  85.1 us (99%)
    pallas_call x1, Pallas kernels, shards(): pl.pallas_call(functools.partial(main_kernel, n, n_tp, chans * n_tp, halo...  82.4 us
    pallas_call x1, Pallas kernels, shards(): pl.pallas_call(finish_kernel, out_shape=(shape((tokens, cols), BF), shape...  2.73 us

profile of v1, /device:TPU:14, one launch (start us, length us, event | category | flops | bytes accessed | tf_op | source)
XLA Modules:
  0.0 85.9 jit_solution(2690450825034838842)
XLA Ops:
  0.6 82.4 %main.1 = (bf16[1024,512]{1,0:T(8,128)(2,1)}, f32[256,512]{1,0:T(8,128)}, f32[256,256]{1,0:T(8,128)}, f32[40,256]{1,0:T(8,128)}) custom-call(bf16[1024,2048]{1,0:T(8,128)(2,1)} %bi_hbm.1, bf16[1024,2048]{1,0:T(8,128)(2,1)} %og_hbm.1, bf16[2048,256]{1,0:T(8,128)(2,1)} %wv_hbm.1, bf16[2048,256]{1,0:T(8,128)(2,1)} %wg_hbm.1, bf16[256,2048]{1,0:T(8,128)(2,1)} %wp_hbm.1, ...), custom_call_target="tpu_custom_call" | custom-call | tf_op jit(solution)/shard_map/main/pallas_call | solution.py:446
  83.0 2.7 %finish.1 = (bf16[1024,512]{1,0:T(8,128)(2,1)}, f32[256,256]{1,0:T(8,128)}, f32[256,256]{1,0:T(8,128)}, f32[256,256]{1,0:T(8,128)}, f32[31,256]{1,0:T(8,128)}, /*index=5*/f32[1,256]{1,0:T(1,128)}, f32[1,256]{1,0:T(1,128)}) custom-call(bf16[1024,512]{1,0:T(8,128)(2,1)} %get-tuple-element.18.ig_ref, f32[256,512]{1,0:T(8,128)} %get-tuple-element.19.ws_ref, ...), custom_call_target="tpu_custom_call" | custom-call | tf_op jit(solution)/shard_map/finish/pallas_call | solution.py:483

commit v2 on v1

v2 whole, which is shorter than its diff:
```python
import functools
import math

import jax
import jax.numpy as jnp
from jax import lax
from jax.experimental import pallas as pl
from jax.experimental.pallas import tpu as pltpu
from jax.sharding import PartitionSpec as P

EPS = 0.05
MESH = pl.DeviceIdType.MESH
LANES = 128
BF, F32 = jnp.bfloat16, jnp.float32


def right_product(left, right):
    return lax.dot_general(
        left, right, (((1,), (1,)), ((), ())), preferred_element_type=F32
    )


def column_product(left, right):
    return lax.dot_general(
        left, right, (((0,), (0,)), ((), ())), preferred_element_type=F32
    )


def main_kernel(
    n, n_tp, n_chan, halo,
    bi_hbm, og_hbm, wv_hbm, wg_hbm, wp_hbm, taps_ref, gain_ref, shift_ref,
    ig_ref, ws_ref, ps_ref, sm_ref,
    bi, og, ww, wp,
    gx, vp, sg, fl, nm, gn, gf, gm, mo, gb, turned, tacc, cols, rowbuf, so, si,
    part, mate_in, low_out, low_in, far_out, far_in,
    xs, xr, ys, yr, acc, small, small_in, small_pair, small_all, small_sum,
    load_sem, st_send, st_recv, hx_send, hx_recv, hf_send, hf_recv,
    mate_send, mate_recv, low_send, low_recv, far_send, far_recv,
    x_send, x_recv, y_send, y_recv, s_send, s_recv, sa_send, sa_recv, sb_send, sb_recv,
):
    me, t = lax.axis_index("sp"), lax.axis_index("tp")
    outer, inner = me // 2, me % 2
    h = n // 2
    mate = 2 * outer + (1 - inner)
    t_near, t_far = t + 1 - 2 * (t % 2), lax.rem(t + n_tp // 2, n_tp)
    t_cross = lax.rem(t_near + n_tp // 2, n_tp)
    tokens, width = bi.shape
    rows, cols_tp = width // n, width // n_tp
    chans, halves = wp.shape[0], ww.shape[0]
    kernel_len = taps_ref.shape[0]
    chunks = xs.shape[0]
    step = tokens // chunks
    block = 64
    per = step // block

    def load(src, dst, i):
        copy = pltpu.make_async_copy(src, dst, load_sem.at[i])
        copy.start()
        return copy

    def piece(r):
        return pl.ds(r * step, step)

    order_in = [chunks - 1] + list(range(chunks - 1))
    load_w = []
    for c in range(halves):
        at = slice(c * LANES, (c + 1) * LANES)
        load_w.append(load(wv_hbm.at[:, at], ww.at[c, :, :LANES], 2 * c))
        load_w.append(load(wg_hbm.at[:, at], ww.at[c, :, LANES:], 2 * c + 1))
    load_bi = {r: load(bi_hbm.at[piece(r)], bi.at[piece(r)], 2 * halves + r) for r in order_in}
    load_wp = load(wp_hbm, wp, 2 * halves + chunks)
    load_og = load(og_hbm, og, 2 * halves + chunks + 1)

    barrier = pltpu.get_barrier_semaphore()
    group = h // 4
    levels = group.bit_length() - 1
    place, low = outer // group, outer % group
    low_flips = [(1 << q) * (1 - 2 * ((low // (1 << q)) % 2)) for q in range(levels)]
    flip_near, flip_far = 1 - 2 * (place % 2), 2 - 4 * (place // 2)
    edge = 1 - (place % 2 + place // 2) % 2
    ends = [
        place + flip_near + edge * flip_far, place + flip_far,
        place + flip_near + (1 - edge) * flip_far, place,
    ]

    def outer_of(spot, mask):
        return spot * group + sum((low_flips[q] for q in range(levels) if mask >> q & 1), low)

    peers = [{"sp": 2 * lax.rem(outer + k, h) + inner} for k in range(1, h)]
    peers += [{"sp": mate}, {"sp": lax.rem(me + 1, n)}, {"sp": lax.rem(me + n - 1, n)}]
    peers += [{"tp": lax.rem(t + k, n_tp)} for k in range(1, n_tp)]
    for who in peers:
        pl.semaphore_signal(barrier, inc=1, device_id=who, device_id_type=MESH)

    first, last = me == 0, me == n - 1
    tacc[...] = jnp.zeros_like(tacc)

    @pl.when(first)
    def _():
        gx[:, :halo, :] = jnp.zeros((halves, halo, LANES), F32)

    @pl.when(last)
    def _():
        gf[:, tokens:, :] = jnp.zeros((halves, halo, LANES), F32)

    def describe(src, dst, send_sem, recv_sem, who):
        return pltpu.make_async_remote_copy(
            src_ref=src, dst_ref=dst, send_sem=send_sem, recv_sem=recv_sem,
            device_id=who, device_id_type=MESH,
        )

    def send(*args):
        copy = describe(*args)
        copy.start()
        return copy

    sent = []

    halo_x = describe(
        gx.at[:, pl.ds(tokens, halo), :], gx.at[:, pl.ds(0, halo), :],
        hx_send.at[0], hx_recv.at[0], {"sp": lax.rem(me + 1, n)},
    )
    for copy in load_w:
        copy.wait()
    for r in order_in:
        load_bi[r].wait()
        where = piece(r)
        for c in range(halves):
            at = slice(c * LANES, (c + 1) * LANES)
            both = jnp.dot(bi[where, :], ww[c], preferred_element_type=F32).astype(BF)
            value = both[:, :LANES]
            sigmoid = jax.nn.sigmoid(both[:, LANES:].astype(F32))
            vp[where, at] = value
            sg[where, at] = sigmoid
            gx[c, pl.ds(halo + r * step, step), :] = (value.astype(F32) * sigmoid).astype(BF).astype(F32)

    pl.semaphore_wait(barrier, len(peers))

    @pl.when(me < n - 1)
    def _():
        halo_x.start()

    load_og.wait()

    lane = lax.broadcasted_iota(jnp.int32, (block, LANES), 1)

    def send_stats(phase, r):
        so[phase, r] = rowbuf[...].T[:8]
        copies = [
            send(so.at[phase, r], si.at[phase, r, k - 1], st_send.at[phase, r, k - 1],
                 st_recv.at[phase, r, k - 1], {"tp": lax.rem(t + k, n_tp)})
            for k in range(1, n_tp)
        ]
        sent.extend(copies)
        return copies

    def take_stats(phase, r, copies):
        total = so[phase, r]
        for k, copy in enumerate(copies):
            copy.wait_recv()
            total = total + si[phase, r, k]
        return total / n_chan

    def rows_of(base, i):
        return pl.ds(pl.multiple_of(base + i * block, block), block)

    def pair_of_sums(i, first_sum, second_sum):
        rowbuf[rows_of(0, i), :] = jnp.where(
            lane == 0, first_sum, jnp.where(lane == 1, second_sum, 0.0)
        )

    def conv_chunk(r):
        def body(i, carry):
            sums = jnp.zeros((block, LANES), F32)
            squares = jnp.zeros((block, LANES), F32)
            for c in range(halves):
                total = jnp.zeros((block, LANES), F32)
                for k in range(kernel_len):
                    where = pl.ds(r * step + i * block + halo - k, block)
                    total = total + taps_ref[pl.ds(k, 1), c * LANES:(c + 1) * LANES] * gx[c, where, :]
                fl[c, rows_of(r * step, i), :] = total
                sums = sums + total
                squares = squares + total * total
            pair_of_sums(i, jnp.sum(sums, axis=1, keepdims=True), jnp.sum(squares, axis=1, keepdims=True))
            return carry

        lax.fori_loop(0, per, body, 0, unroll=2)
        return send_stats(0, r)

    late_first = list(range(1, chunks)) + [0]
    moments, means = {}, {}
    for r in late_first:
        if r == 0:
            @pl.when(me > 0)
            def _():
                halo_x.wait_recv()
        moments[r] = conv_chunk(r)

    def norm_chunk(r):
        total = take_stats(0, r, moments[r])
        mean = total[0:1]
        scale = lax.rsqrt(total[1:2] - mean * mean + EPS)
        both = jnp.where(lax.broadcasted_iota(jnp.int32, total.shape, 0) == 0, mean, scale)
        cols[0, piece(r), :8] = both.T

        def body(i, carry):
            where = rows_of(r * step, i)
            mean = cols[0, where, 0:1]
            scale = cols[0, where, 1:2]
            for c in range(halves):
                at = slice(c * LANES, (c + 1) * LANES)
                normed = (fl[c, where, :] - mean) * scale
                activated = normed * gain_ref[:, at] + shift_ref[:, at]
                sigmoid = jax.nn.sigmoid(activated)
                mo[where, at] = (activated * sigmoid).astype(BF)
                nm[c, where, :] = normed
                fl[c, where, :] = sigmoid
            return carry

        lax.fori_loop(0, per, body, 0, unroll=True)

    def cotangent_chunk(r, carry):
        def body(i, carry):
            where = rows_of(r * step, i)
            sums = jnp.zeros((block, LANES), F32)
            crosses = jnp.zeros((block, LANES), F32)
            out = []
            for c in range(halves):
                at = slice(c * LANES, (c + 1) * LANES)
                gain = gain_ref[:, at]
                normed = nm[c, where, :]
                activated = normed * gain + shift_ref[:, at]
                sigmoid = fl[c, where, :]
                grad_act = gm[where, at] * sigmoid * (1.0 + activated * (1.0 - sigmoid))
                grad_normed = grad_act * gain
                gn[c, where, :] = grad_normed
                sums = sums + grad_normed
                crosses = crosses + grad_normed * normed
                fold = lambda x: x.reshape(block // 8, 8, LANES).sum(axis=0)
                out.append(carry[2 * c] + fold(grad_act * normed))
                out.append(carry[2 * c + 1] + fold(grad_act))
            pair_of_sums(i, jnp.sum(sums, axis=1, keepdims=True), jnp.sum(crosses, axis=1, keepdims=True))
            return tuple(out)

        carry = lax.fori_loop(0, per, body, carry, unroll=True)
        return send_stats(1, r), carry

    for r in late_first:
        norm_chunk(r)

    aligned = rows % LANES == 0
    wide = 256

    blocks_of = [(mask, i) for mask in range(group - 1, -1, -1) for i in range(4)]
    acts = [og] + [bi] * halves
    mate_copies = [[] for _ in acts]
    low_copies = [{} for _ in acts]
    far_copies = [[] for _ in acts]

    def device_block(k, i):
        mask, spot = blocks_of[k]
        return 2 * outer_of(ends[spot], mask) + i

    def make_others(j, other):
        if aligned:
            turned[j] = other.T
        else:
            for w in range(width // wide):
                found = column_product(acts[j][:, w * wide:(w + 1) * wide], other).astype(BF)
                part[j, pl.ds(w * (wide // rows), wide // rows)] = found.reshape(wide // rows, rows, found.shape[1])

    def product(j, b):
        where = pl.ds(pl.multiple_of(b * rows, rows), rows)
        return jnp.dot(turned[j], acts[j][:, where], preferred_element_type=F32)

    def make_mates(j, ks):
        blocks = [device_block(k, 1 - inner) for k in ks]
        if aligned:
            found = [product(j, b) for b in blocks]
            for b, block in zip(blocks, found):
                part[j, b] = block.astype(BF)

    def send_mates(j, ks):
        for k in ks:
            b = device_block(k, 1 - inner)
            mate_copies[j].append(send(
                part.at[j, b], mate_in.at[j, k], mate_send.at[j, k], mate_recv.at[j, k], {"sp": mate}
            ))

    pairs = [range(k, min(k + 2, h)) for k in range(0, h, 2)]

    def mate_blocks(j):
        for ks in pairs:
            make_mates(j, ks)
            send_mates(j, ks)

    def landed(j, slot):
        return describe(
            far_out.at[j, 0], far_in.at[j, slot], far_send.at[j, 0], far_recv.at[j, slot], {"sp": mate}
        )

    def far_step(j, k):
        mask, i = blocks_of[k]
        b = device_block(k, inner)
        total = product(j, b) if aligned else part[j, b].astype(F32)
        mate_copies[j][k].wait_recv()
        total = total + mate_in[j, k].astype(F32)
        lowest = [q for q in range(levels) if mask >> q & 1][:1] or [levels]
        for q in range(lowest[0]):
            came = mask + (1 << q)
            low_copies[j][came, i].wait_recv()
            total = total + low_in[j, (came - 1) * 4 + i].astype(F32)
        if mask:
            at = (mask - 1) * 4 + i
            low_out[j, at] = total.astype(BF)
            low_copies[j][mask, i] = send(
                low_out.at[j, at], low_in.at[j, at], low_send.at[j, at], low_recv.at[j, at],
                {"sp": 2 * outer_of(place, 1 << lowest[0]) + inner},
            )
            return
        if i == 3:
            for slot in (2, 3):
                landed(j, slot).wait_recv()
                total = total + far_in[j, slot].astype(F32)
            return total
        if i:
            @pl.when(edge == 0)
            def _():
                landed(j, i - 1).wait_recv()
                far_out[j, i] = (total + far_in[j, i - 1].astype(F32)).astype(BF)

            @pl.when(edge == 1)
            def _():
                far_out[j, i] = total.astype(BF)

            slot = edge * i + (1 - edge) * 3
            target = edge * (place + flip_near) + (1 - edge) * ends[i]
        else:
            far_out[j, i] = total.astype(BF)
            slot, target = (1 - edge) * 2, place + flip_near
        far_copies[j].append(send(
            far_out.at[j, i], far_in.at[j, slot], far_send.at[j, i], far_recv.at[j, slot],
            {"sp": 2 * outer_of(target, 0) + inner},
        ))

    make_others(0, mo[...])
    make_mates(0, pairs[0])
    send_mates(0, pairs[0])

    load_wp.wait()
    carry = tuple(jnp.zeros((8, LANES), F32) for _ in range(2 * halves))
    for r in range(0, chunks, 2):
        mixed = [right_product(og[piece(i), :], wp[...]) for i in (r, r + 1)]
        gm[piece(r), :] = mixed[0]
        gm[piece(r + 1), :] = mixed[1]
        for i in (r, r + 1):
            means[i], carry = cotangent_chunk(i, carry)
    for ks in pairs[1:]:
        make_mates(0, ks)
    small[...] = jnp.zeros_like(small)
    for c in range(halves):
        small[c, kernel_len:kernel_len + 1] = carry[2 * c].sum(axis=0, keepdims=True)
        small[c, kernel_len + 1:kernel_len + 2] = carry[2 * c + 1].sum(axis=0, keepdims=True)

    halo_f = describe(
        gf.at[:, pl.ds(0, halo), :], gf.at[:, pl.ds(tokens, halo), :],
        hf_send.at[0], hf_recv.at[0], {"sp": lax.rem(me + n - 1, n)},
    )

    def filtered_chunk(r):
        cols[1, piece(r), :8] = take_stats(1, r, means[r]).T

        def body(i, carry):
            where = rows_of(r * step, i)
            scale = cols[0, where, 1:2]
            first_mean = cols[1, where, 0:1]
            second_mean = cols[1, where, 1:2]
            for c in range(halves):
                gf[c, where, :] = scale * (
                    gn[c, where, :] - first_mean - nm[c, where, :] * second_mean
                )
            return carry

        lax.fori_loop(0, per, body, 0, unroll=True)

    def back_chunk(r, c):
        at = slice(c * LANES, (c + 1) * LANES)

        def body(i, carry):
            where = rows_of(r * step, i)
            gated = gx[c, pl.ds(pl.multiple_of(r * step + i * block + halo, 8), block), :]
            total = jnp.zeros((block, LANES), F32)
            for k in range(kernel_len):
                grad = gf[c, pl.ds(r * step + i * block + k, block), :]
                total = total + taps_ref[pl.ds(k, 1), at] * grad
                tacc[c, k] += (gated * grad).reshape(block // 8, 8, LANES).sum(axis=0)
            sigmoid = sg[where, at]
            value = vp[where, at].astype(F32)
            gb[c, where, :LANES] = (total * sigmoid).astype(BF)
            gb[c, where, LANES:] = (total * value * sigmoid * (1.0 - sigmoid)).astype(BF)
            return carry

        lax.fori_loop(0, per, body, 0)

    def partial_input(r, j):
        at = pl.ds(pl.multiple_of(j * cols_tp, cols_tp), cols_tp)
        total = right_product(gb[0, piece(r), :], ww[0, at, :])
        for c in range(1, halves):
            total = total + right_product(gb[c, piece(r), :], ww[c, at, :])
        return total

    x_copies, y_copies = [], []

    def near_block(r):
        xs[r, 0] = partial_input(r, t_cross).astype(BF)
        xs[r, 1] = partial_input(r, t_near).astype(BF)
        x_copies.append(send(xs.at[r], xr.at[r], x_send.at[r], x_recv.at[r], {"tp": t_near}))

    def far_block(r):
        far = partial_input(r, t_far)
        acc[piece(r), :] = partial_input(r, t)
        x_copies[r].wait_recv()
        ys[r] = (far + xr[r, 0].astype(F32)).astype(BF)
        y_copies.append(send(ys.at[r], yr.at[r], y_send.at[r], y_recv.at[r], {"tp": t_far}))
        acc[piece(r), :] += xr[r, 1].astype(F32)

    filtered_chunk(0)

    @pl.when(me > 0)
    def _():
        halo_f.start()

    for ks in pairs[1:]:
        send_mates(0, ks)
    todo = [(j, k) for j in range(1 + halves) for k in range(h - 1)]
    far_step(*todo.pop(0))
    for r in range(1, chunks):
        filtered_chunk(r)


    def far_steps(count):
        for _ in range(count):
            far_step(*todo.pop(0))

    for c in range(halves):
        for r in range(chunks):
            if c == 0 and r == chunks - 1:
                @pl.when(me < n - 1)
                def _():
                    halo_f.wait_recv()
            back_chunk(r, c)
            if c == halves - 1:
                near_block(r)
                if r:
                    far_block(r - 1)
                if r > 1:
                    far_steps(1)
        small[c, :kernel_len] = tacc[c].sum(axis=1)
        if c == halves - 1:
            small_copy = send(small.at[1 - inner], small_in, s_send.at[0], s_recv.at[0], {"sp": mate})
        make_others(1 + c, gb[c])
        mate_blocks(1 + c)
        if c == 0:
            far_steps(1)
    far_block(chunks - 1)

    loss_scale = 1.0 / math.sqrt(tokens * n)
    far_steps(len(todo) - (h - 1))
    small_copy.wait_recv()
    small_pair[...] = small[inner] + small_in[...]
    small_copies = [
        send(small_pair, small_all.at[outer], sa_send.at[k - 1], sa_recv.at[k - 1],
             {"sp": 2 * lax.rem(outer + k, h) + inner})
        for k in range(1, h)
    ]
    far_steps(len(todo) - 1)
    for copy in small_copies:
        copy.wait_recv()
    small_all[outer] = small_pair[...]
    total = small_all[0]
    for k in range(1, h):
        total = total + small_all[k]
    small_sum[inner] = total * loss_scale
    half_copy = send(
        small_sum.at[inner], small_sum.at[inner], sb_send.at[0], sb_recv.at[0], {"sp": mate}
    )
    far_steps(1)

    total = far_step(0, h - 1) * loss_scale
    ps_ref[...] = total if aligned else total.T
    for r in range(chunks):
        y_copies[r].wait_recv()
        ig_ref[piece(r), :] = (acc[piece(r), :] + yr[r].astype(F32)).astype(BF)
    for c in range(halves):
        total = far_step(1 + c, h - 1) * loss_scale
        ws_ref[c] = total.T if aligned else total
    half_copy.wait_recv()
    sm_ref[...] = small_sum[...]

    @pl.when(me < n - 1)
    def _():
        halo_x.wait_send()

    @pl.when(me > 0)
    def _():
        halo_f.wait_send()

    for copies in mate_copies + far_copies + [list(found.values()) for found in low_copies]:
        sent.extend(copies)
    for copy in sent + x_copies + y_copies + small_copies + [small_copy, half_copy]:
        copy.wait_send()


def finish_kernel(
    ig_ref, ws_ref, ps_ref, sm_ref, ig_out, wv_out, wg_out, wp_out, taps_out, gain_out, shift_out,
    taps, gain, shift, sems,
):
    chans = ps_ref.shape[0]
    kernel_len = taps_out.shape[0]
    copies = []

    def store(src, dst):
        copies.append(pltpu.make_async_copy(src, dst, sems.at[len(copies)]))
        copies[-1].start()

    store(ig_ref, ig_out)
    store(ps_ref, wp_out)
    for c in range(chans // LANES):
        at = slice(c * LANES, (c + 1) * LANES)
        store(ws_ref.at[c, :, :LANES], wv_out.at[:, at])
        store(ws_ref.at[c, :, LANES:], wg_out.at[:, at])
        taps[:, at] = sm_ref[c, :kernel_len]
        gain[:, at] = sm_ref[c, kernel_len:kernel_len + 1]
        shift[:, at] = sm_ref[c, kernel_len + 1:kernel_len + 2]
    store(taps, taps_out)
    store(gain, gain_out)
    store(shift, shift_out)
    for copy in copies:
        copy.wait()


def shards(block_input, out_grad, w_value, w_gate, conv_taps, norm_gain, norm_shift, w_proj):
    n, n_tp = lax.axis_size("sp"), lax.axis_size("tp")
    tokens, width = block_input.shape
    chans = w_value.shape[1]
    kernel_len = conv_taps.shape[0]
    halves = chans // LANES
    halo = -(-(kernel_len - 1) // 8) * 8
    rows, cols, h, chunks = width // n, width // n_tp, n // 2, 4
    step = tokens // chunks
    smalls = (-(-(kernel_len + 2) // 8) * 8, LANES)
    pair, sums, lows = 2 * LANES, 1 + halves, max(h - 4, 1)
    part = (pair, rows) if rows % LANES == 0 else (rows, pair)
    anywhere = pl.BlockSpec(memory_space=pl.ANY)
    vmem = pl.BlockSpec(memory_space=pltpu.VMEM)
    dma = pltpu.SemaphoreType.DMA
    V = pltpu.VMEM
    shape = jax.ShapeDtypeStruct
    results = pl.pallas_call(
        functools.partial(main_kernel, n, n_tp, chans * n_tp, halo),
        out_shape=(
            shape((tokens, cols), BF), shape((halves, rows, pair), F32),
            shape((chans, rows), F32), shape((halves,) + smalls, F32),
        ),
        in_specs=[pl.BlockSpec(memory_space=pltpu.HBM)] * 5 + [vmem] * 3,
        out_specs=(vmem,) * 4,
        scratch_shapes=[
            V((tokens, width), BF), V((tokens, width), BF), V((halves, width, pair), BF),
            V((chans, width), BF),
            V((halves, halo + tokens, LANES), F32), V((tokens, chans), BF), V((tokens, chans), F32),
            V((halves, tokens, LANES), F32), V((halves, tokens, LANES), F32), V((halves, tokens, LANES), F32),
            V((halves, tokens + halo, LANES), F32), V((tokens, chans), F32), V((tokens, chans), BF),
            V((halves, tokens, pair), BF), V((sums, pair, tokens), BF), V((halves, kernel_len, 8, LANES), F32), V((2, tokens, LANES), F32),
            V((step, LANES), F32), V((2, chunks, 8, step), F32), V((2, chunks, n_tp - 1, 8, step), F32),
            V((sums, n) + part, BF), V((sums, h) + part, BF), V((sums, lows) + part, BF), V((sums, lows) + part, BF),
            V((sums, 3) + part, BF), V((sums, 4) + part, BF),
            V((chunks, 2, step, cols), BF), V((chunks, 2, step, cols), BF), V((chunks, step, cols), BF),
            V((chunks, step, cols), BF), V((tokens, cols), F32),
            V((halves,) + smalls, F32), V(smalls, F32), V(smalls, F32), V((h,) + smalls, F32),
            V((halves,) + smalls, F32),
            dma((2 * halves + chunks + 2,)), dma((2, chunks, n_tp - 1)), dma((2, chunks, n_tp - 1)),
            dma((1,)), dma((1,)), dma((1,)), dma((1,)),
            dma((sums, h)), dma((sums, h)), dma((sums, lows)), dma((sums, lows)), dma((sums, 3)), dma((sums, 4)),
            dma((chunks,)), dma((chunks,)), dma((chunks,)), dma((chunks,)), dma((1,)), dma((1,)),
            dma((h - 1,)), dma((h - 1,)), dma((1,)), dma((1,)),
        ],
        compiler_params=pltpu.CompilerParams(
            collective_id=0, has_side_effects=True, vmem_limit_bytes=52 * 1024 * 1024
        ),
        name="main",
    )(
        block_input, out_grad, w_value, w_gate, w_proj, conv_taps,
        norm_gain.reshape(1, chans), norm_shift.reshape(1, chans),
    )
    outs = pl.pallas_call(
        finish_kernel,
        out_shape=(
            shape((tokens, cols), BF), shape((rows, chans), F32), shape((rows, chans), F32),
            shape((chans, rows), F32), shape((kernel_len, chans), F32), shape((1, chans), F32), shape((1, chans), F32),
        ),
        in_specs=[vmem] * 4,
        out_specs=(anywhere,) * 7,
        scratch_shapes=[
            V((kernel_len, chans), F32), V((1, chans), F32), V((1, chans), F32), dma((5 + 2 * halves,)),
        ],
        compiler_params=pltpu.CompilerParams(vmem_limit_bytes=4 * 1024 * 1024),
        name="finish",
    )(*results)
    return outs[:5] + (outs[5].reshape(chans), outs[6].reshape(chans))


def solution(mesh):
    return jax.shard_map(
        shards,
        mesh=mesh,
        in_specs=(
            P("sp", None),
            P("sp", None),
            P(None, "tp"),
            P(None, "tp"),
            P(None, "tp"),
            P("tp"),
            P("tp"),
            P("tp", None),
        ),
        out_specs=(
            P("sp", "tp"),
            P("sp", "tp"),
            P("sp", "tp"),
            P("tp", "sp"),
            P(None, "tp"),
            P("tp"),
            P("tp"),
        ),
        check_vma=False,
    )
```

time: 86.1 us -> 61.5 us (0.71)
  the two profiles are of different devices: /device:TPU:14 before, /device:TPU:0 now
where the time goes in v2:
time: 61.5 us; the launch traced here: 61.2 us
  Pallas kernels  58.3 us (95%)
  local copies, waits for them, and re-layouts  2.11 us (3%)
  between operations  0.81 us (1%)
    pallas_call x1, Pallas kernels, shards(): pl.pallas_call(functools.partial(main_kernel, n, n_tp, chans * n_tp, halo...  57 us
    unnamed x6, local copies, waits for them, and re-layouts  2.11 us
    pallas_call x1, Pallas kernels, shards(): pl.pallas_call(finish_kernel, out_shape=(shape((tokens, cols), BF), shape...  1.3 us

profile of v2, /device:TPU:0, one launch (start us, length us, event | category | flops | bytes accessed | tf_op | source)
XLA Modules:
  0.0 61.2 jit_solution(18287435271993729282)
XLA Ops:
  0.6 0.0 copy-start
  0.6 0.7 %copy-done = f32[31,256]{1,0:T(8,128)S(1)} copy-done((f32[31,256]{1,0:T(8,128)S(1)}, f32[31,256]{1,0:T(8,128)}, u32[]{:S(2)}) %copy-start) | copy-done | bytes 31768
  1.4 0.0 copy-start.1
  1.4 0.7 %copy-done.1 = f32[256]{0:T(256)S(1)} copy-done((f32[256]{0:T(256)S(1)}, f32[256]{0:T(256)}, u32[]{:S(2)}) %copy-start.1) | copy-done | bytes 1048
  2.1 0.0 copy-start.2
  2.1 0.7 %copy-done.2 = f32[256]{0:T(256)S(1)} copy-done((f32[256]{0:T(256)S(1)}, f32[256]{0:T(256)}, u32[]{:S(2)}) %copy-start.2) | copy-done | bytes 1048
  2.8 57.0 %main.1 = (bf16[1024,512]{1,0:T(8,128)(2,1)S(1)}, f32[2,256,256]{2,1,0:T(8,128)S(1)}, f32[256,256]{1,0:T(8,128)S(1)}, f32[2,40,128]{2,1,0:T(8,128)S(1)}) custom-call(bf16[1024,2048]{1,0:T(8,128)(2,1)} %bi_hbm.1, bf16[1024,2048]{1,0:T(8,128)(2,1)} %og_hbm.1, bf16[2048,256]{1,0:T(8,128)(2,1)} %wv_hbm.1, bf16[2048,256]{1,0:T(8,128)(2,1)} %wg_hbm.1, ...), custom_call_target="tpu_custom_call" | custom-call | tf_op jit(solution)/shard_map/main/pallas_call | solution.py:559
  59.8 1.3 %finish.1 = (bf16[1024,512]{1,0:T(8,128)(2,1)}, f32[256,256]{1,0:T(8,128)}, f32[256,256]{1,0:T(8,128)}, f32[256,256]{1,0:T(8,128)}, f32[31,256]{1,0:T(8,128)}, /*index=5*/f32[1,256]{1,0:T(1,128)}, f32[1,256]{1,0:T(1,128)}) custom-call(bf16[1024,512]{1,0:T(8,128)(2,1)S(1)} %get-tuple-element.18.ig_ref, f32[2,256,256]{2,1,0:T(8,128)S(1)} %get-tuple-element.19.ws_ref, ...), custom_call_target="tpu_custom_call" | custom-call | tf_op jit(solution)/shard_map/finish/pallas_call | solution.py:595
Async XLA Ops:
  0.6 0.8 %copy-start = (f32[31,256]{1,0:T(8,128)S(1)}, f32[31,256]{1,0:T(8,128)}, u32[]{:S(2)}) copy-start(f32[31,256]{1,0:T(8,128)} %taps_ref.1) | copy-start | bytes 95236
  1.4 0.7 %copy-start.1 = (f32[256]{0:T(256)S(1)}, f32[256]{0:T(256)}, u32[]{:S(2)}) copy-start(f32[256]{0:T(256)} %param.13) | copy-start | bytes 3076
  2.1 0.7 %copy-start.2 = (f32[256]{0:T(256)S(1)}, f32[256]{0:T(256)}, u32[]{:S(2)}) copy-start(f32[256]{0:T(256)} %param.14) | copy-start | bytes 3076

commit v3 on v2

--- a/solution.py
+++ b/solution.py
@@ -28,11 +28,11 @@
 
 def main_kernel(
     n, n_tp, n_chan, halo,
-    bi_hbm, og_hbm, wv_hbm, wg_hbm, wp_hbm, taps_ref, gain_ref, shift_ref,
+    bi_hbm, og_hbm, wv_hbm, wg_hbm, wp_hbm, taps_hbm, gain_hbm, shift_hbm,
     ig_ref, ws_ref, ps_ref, sm_ref,
-    bi, og, ww, wp,
+    bi, og, ww, wp, taps_ref, gain_ref, shift_ref,
     gx, vp, sg, fl, nm, gn, gf, gm, mo, gb, turned, tacc, cols, rowbuf, so, si,
-    part, mate_in, low_out, low_in, far_out, far_in,
+    part, own, mate_in, low_out, low_in, far_out, far_in,
     xs, xr, ys, yr, acc, small, small_in, small_pair, small_all, small_sum,
     load_sem, st_send, st_recv, hx_send, hx_recv, hf_send, hf_recv,
     mate_send, mate_recv, low_send, low_recv, far_send, far_recv,
@@ -67,9 +67,10 @@
         at = slice(c * LANES, (c + 1) * LANES)
         load_w.append(load(wv_hbm.at[:, at], ww.at[c, :, :LANES], 2 * c))
         load_w.append(load(wg_hbm.at[:, at], ww.at[c, :, LANES:], 2 * c + 1))
-    load_bi = {r: load(bi_hbm.at[piece(r)], bi.at[piece(r)], 2 * halves + r) for r in order_in}
-    load_wp = load(wp_hbm, wp, 2 * halves + chunks)
-    load_og = load(og_hbm, og, 2 * halves + chunks + 1)
+    def load_input(r):
+        return load(bi_hbm.at[piece(r)], bi.at[piece(r)], 2 * halves + r)
+
+    load_bi = {order_in[0]: load_input(order_in[0])}
 
     barrier = pltpu.get_barrier_semaphore()
     group = h // 4
@@ -122,8 +123,17 @@
     )
     for copy in load_w:
         copy.wait()
+    for r in order_in[1:]:
+        load_bi[r] = load_input(r)
+    at_sem = 2 * halves + chunks
+    load_small = [
+        load(src, dst, at_sem + 2 + i)
+        for i, (src, dst) in enumerate(((taps_hbm, taps_ref), (gain_hbm, gain_ref), (shift_hbm, shift_ref)))
+    ]
     for r in order_in:
         load_bi[r].wait()
+        if r == order_in[1]:
+            load_og, load_wp = load(og_hbm, og, at_sem + 1), load(wp_hbm, wp, at_sem)
         where = piece(r)
         for c in range(halves):
             at = slice(c * LANES, (c + 1) * LANES)
@@ -140,7 +150,8 @@
     def _():
         halo_x.start()
 
-    load_og.wait()
+    for copy in load_small:
+        copy.wait()
 
     lane = lax.broadcasted_iota(jnp.int32, (block, LANES), 1)
 
@@ -184,7 +195,7 @@
             pair_of_sums(i, jnp.sum(sums, axis=1, keepdims=True), jnp.sum(squares, axis=1, keepdims=True))
             return carry
 
-        lax.fori_loop(0, per, body, 0, unroll=2)
+        lax.fori_loop(0, per, body, 0, unroll=True)
         return send_stats(0, r)
 
     late_first = list(range(1, chunks)) + [0]
@@ -245,6 +256,14 @@
         carry = lax.fori_loop(0, per, body, carry, unroll=True)
         return send_stats(1, r), carry
 
+    def mix(r):
+        mixed = [right_product(og[piece(i), :], wp[...]) for i in (r, r + 1)]
+        gm[piece(r), :] = mixed[0]
+        gm[piece(r + 1), :] = mixed[1]
+
+    load_wp.wait()
+    load_og.wait()
+    mix(0)
     for r in late_first:
         norm_chunk(r)
 
@@ -292,7 +311,7 @@
     def mate_blocks(j):
         for ks in pairs:
             make_mates(j, ks)
-            send_mates(j, ks)
+            send_mates(j, [k for k in ks if k < h - 1])
 
     def landed(j, slot):
         return describe(
@@ -319,10 +338,8 @@
             )
             return
         if i == 3:
-            for slot in (2, 3):
-                landed(j, slot).wait_recv()
-                total = total + far_in[j, slot].astype(F32)
-            return total
+            own[j] = total
+            return
         if i:
             @pl.when(edge == 0)
             def _():
@@ -343,16 +360,21 @@
             {"sp": 2 * outer_of(target, 0) + inner},
         ))
 
+    def whole(j):
+        total = own[j]
+        for slot in (2, 3):
+            landed(j, slot).wait_recv()
+            total = total + far_in[j, slot].astype(F32)
+        return total * loss_scale
+
     make_others(0, mo[...])
     make_mates(0, pairs[0])
     send_mates(0, pairs[0])
 
-    load_wp.wait()
     carry = tuple(jnp.zeros((8, LANES), F32) for _ in range(2 * halves))
     for r in range(0, chunks, 2):
-        mixed = [right_product(og[piece(i), :], wp[...]) for i in (r, r + 1)]
-        gm[piece(r), :] = mixed[0]
-        gm[piece(r + 1), :] = mixed[1]
+        if r:
+            mix(r)
         for i in (r, r + 1):
             means[i], carry = cotangent_chunk(i, carry)
     for ks in pairs[1:]:
@@ -433,7 +455,6 @@
     for ks in pairs[1:]:
         send_mates(0, ks)
     todo = [(j, k) for j in range(1 + halves) for k in range(h - 1)]
-    far_step(*todo.pop(0))
     for r in range(1, chunks):
         filtered_chunk(r)
 
@@ -443,17 +464,22 @@
             far_step(*todo.pop(0))
 
     for c in range(halves):
-        for r in range(chunks):
+        back_chunk(0, c)
+    far_steps(1)
+    near_block(0)
+    for c in range(halves):
+        for r in range(1, chunks):
             if c == 0 and r == chunks - 1:
                 @pl.when(me < n - 1)
                 def _():
                     halo_f.wait_recv()
             back_chunk(r, c)
+            if c == 0 and r == 1:
+                far_block(0)
             if c == halves - 1:
                 near_block(r)
-                if r:
+                if r > 1:
                     far_block(r - 1)
-                if r > 1:
                     far_steps(1)
         small[c, :kernel_len] = tacc[c].sum(axis=1)
         if c == halves - 1:
@@ -462,9 +488,19 @@
         mate_blocks(1 + c)
         if c == 0:
             far_steps(1)
+    for c in range(halves):
+        send_mates(1 + c, [h - 1])
     far_block(chunks - 1)
 
     loss_scale = 1.0 / math.sqrt(tokens * n)
+    def input_chunk(r):
+        y_copies[r].wait_recv()
+        ig_ref[piece(r), :] = (acc[piece(r), :] + yr[r].astype(F32)).astype(BF)
+
+    def weight_half(c):
+        total = whole(1 + c)
+        ws_ref[c] = total.T if aligned else total
+
     far_steps(len(todo) - (h - 1))
     small_copy.wait_recv()
     small_pair[...] = small[inner] + small_in[...]
@@ -473,6 +509,9 @@
              {"sp": 2 * lax.rem(outer + k, h) + inner})
         for k in range(1, h)
     ]
+    far_step(0, h - 1)
+    total = whole(0)
+    ps_ref[...] = total if aligned else total.T
     far_steps(len(todo) - 1)
     for copy in small_copies:
         copy.wait_recv()
@@ -484,16 +523,13 @@
     half_copy = send(
         small_sum.at[inner], small_sum.at[inner], sb_send.at[0], sb_recv.at[0], {"sp": mate}
     )
+    for r in range(chunks - 1):
+        input_chunk(r)
     far_steps(1)
-
-    total = far_step(0, h - 1) * loss_scale
-    ps_ref[...] = total if aligned else total.T
-    for r in range(chunks):
-        y_copies[r].wait_recv()
-        ig_ref[piece(r), :] = (acc[piece(r), :] + yr[r].astype(F32)).astype(BF)
+    input_chunk(chunks - 1)
     for c in range(halves):
-        total = far_step(1 + c, h - 1) * loss_scale
-        ws_ref[c] = total.T if aligned else total
+        far_step(1 + c, h - 1)
+        weight_half(c)
     half_copy.wait_recv()
     sm_ref[...] = small_sum[...]
 
@@ -562,23 +598,23 @@
             shape((tokens, cols), BF), shape((halves, rows, pair), F32),
             shape((chans, rows), F32), shape((halves,) + smalls, F32),
         ),
-        in_specs=[pl.BlockSpec(memory_space=pltpu.HBM)] * 5 + [vmem] * 3,
+        in_specs=[pl.BlockSpec(memory_space=pltpu.HBM)] * 8,
         out_specs=(vmem,) * 4,
         scratch_shapes=[
             V((tokens, width), BF), V((tokens, width), BF), V((halves, width, pair), BF),
-            V((chans, width), BF),
+            V((chans, width), BF), V((kernel_len, chans), F32), V((1, chans), F32), V((1, chans), F32),
             V((halves, halo + tokens, LANES), F32), V((tokens, chans), BF), V((tokens, chans), F32),
             V((halves, tokens, LANES), F32), V((halves, tokens, LANES), F32), V((halves, tokens, LANES), F32),
             V((halves, tokens + halo, LANES), F32), V((tokens, chans), F32), V((tokens, chans), BF),
             V((halves, tokens, pair), BF), V((sums, pair, tokens), BF), V((halves, kernel_len, 8, LANES), F32), V((2, tokens, LANES), F32),
             V((step, LANES), F32), V((2, chunks, 8, step), F32), V((2, chunks, n_tp - 1, 8, step), F32),
-            V((sums, n) + part, BF), V((sums, h) + part, BF), V((sums, lows) + part, BF), V((sums, lows) + part, BF),
+            V((sums, n) + part, BF), V((sums,) + part, F32), V((sums, h) + part, BF), V((sums, lows) + part, BF), V((sums, lows) + part, BF),
             V((sums, 3) + part, BF), V((sums, 4) + part, BF),
             V((chunks, 2, step, cols), BF), V((chunks, 2, step, cols), BF), V((chunks, step, cols), BF),
             V((chunks, step, cols), BF), V((tokens, cols), F32),
             V((halves,) + smalls, F32), V(smalls, F32), V(smalls, F32), V((h,) + smalls, F32),
             V((halves,) + smalls, F32),
-            dma((2 * halves + chunks + 2,)), dma((2, chunks, n_tp - 1)), dma((2, chunks, n_tp - 1)),
+            dma((2 * halves + chunks + 5,)), dma((2, chunks, n_tp - 1)), dma((2, chunks, n_tp - 1)),
             dma((1,)), dma((1,)), dma((1,)), dma((1,)),
             dma((sums, h)), dma((sums, h)), dma((sums, lows)), dma((sums, lows)), dma((sums, 3)), dma((sums, 4)),
             dma((chunks,)), dma((chunks,)), dma((chunks,)), dma((chunks,)), dma((1,)), dma((1,)),
@@ -588,10 +624,13 @@
             collective_id=0, has_side_effects=True, vmem_limit_bytes=52 * 1024 * 1024
         ),
         name="main",
-    )(
-        block_input, out_grad, w_value, w_gate, w_proj, conv_taps,
-        norm_gain.reshape(1, chans), norm_shift.reshape(1, chans),
-    )
+    )(*[
+        pltpu.with_memory_space_constraint(x, pltpu.HBM)
+        for x in (
+            block_input, out_grad, w_value, w_gate, w_proj, conv_taps,
+            norm_gain.reshape(1, chans), norm_shift.reshape(1, chans),
+        )
+    ])
     outs = pl.pallas_call(
         finish_kernel,
         out_shape=(

time: 61.5 us -> 57.4 us (0.933)
  local copies, waits for them, and re-layouts: 2.11 us -> 0 us
  Pallas kernels: 58.3 us -> 56.2 us
    pallas_call x1, Pallas kernels: 57 us -> 54.9 us  [shards(): pl.pallas_call(functools.partial(main_kernel, n, n_tp, chans * n_tp, halo...]
    unnamed x6 -> x0, local copies, waits for them, and re-layouts: 2.11 us -> none
where the time goes in v3:
time: 57.4 us; the launch traced here: 57 us
  Pallas kernels  56.2 us (98%)
  between operations  0.8 us (1%)
    pallas_call x1, Pallas kernels, shards(): pl.pallas_call(functools.partial(main_kernel, n, n_tp, chans * n_tp, halo...  54.9 us
    pallas_call x1, Pallas kernels, shards(): pl.pallas_call(finish_kernel, out_shape=(shape((tokens, cols), BF), shape...  1.3 us

profile of v3, /device:TPU:0, one launch (start us, length us, event | category | flops | bytes accessed | tf_op | source)
XLA Modules:
  0.0 57.0 jit_solution(4509350086243929650)
XLA Ops:
  0.6 54.9 %main.1 = (bf16[1024,512]{1,0:T(8,128)(2,1)S(1)}, f32[2,256,256]{2,1,0:T(8,128)S(1)}, f32[256,256]{1,0:T(8,128)S(1)}, f32[2,40,128]{2,1,0:T(8,128)S(1)}) custom-call(bf16[1024,2048]{1,0:T(8,128)(2,1)} %bi_hbm.1, bf16[1024,2048]{1,0:T(8,128)(2,1)} %og_hbm.1, bf16[2048,256]{1,0:T(8,128)(2,1)} %wv_hbm.1, bf16[2048,256]{1,0:T(8,128)(2,1)} %wg_hbm.1, ...), custom_call_target="tpu_custom_call" | custom-call | tf_op jit(solution)/shard_map/main/pallas_call | solution.py:595
  55.5 1.3 %finish.1 = (bf16[1024,512]{1,0:T(8,128)(2,1)}, f32[256,256]{1,0:T(8,128)}, f32[256,256]{1,0:T(8,128)}, f32[256,256]{1,0:T(8,128)}, f32[31,256]{1,0:T(8,128)}, /*index=5*/f32[1,256]{1,0:T(1,128)}, f32[1,256]{1,0:T(1,128)}) custom-call(bf16[1024,512]{1,0:T(8,128)(2,1)S(1)} %get-tuple-element.18.ig_ref, f32[2,256,256]{2,1,0:T(8,128)S(1)} %get-tuple-element.19.ws_ref, ...), custom_call_target="tpu_custom_call" | custom-call | tf_op jit(solution)/shard_map/finish/pallas_call | solution.py:634

commit v4 on v3

--- a/solution.py
+++ b/solution.py
@@ -143,12 +143,13 @@
             vp[where, at] = value
             sg[where, at] = sigmoid
             gx[c, pl.ds(halo + r * step, step), :] = (value.astype(F32) * sigmoid).astype(BF).astype(F32)
-
-    pl.semaphore_wait(barrier, len(peers))
-
-    @pl.when(me < n - 1)
-    def _():
-        halo_x.start()
+        if r == order_in[0]:
+            pl.semaphore_wait(barrier, len(peers))
+
+            @pl.when(me < n - 1)
+            def _():
+                halo_x.start()
+
 
     for copy in load_small:
         copy.wait()
@@ -198,9 +199,9 @@
         lax.fori_loop(0, per, body, 0, unroll=True)
         return send_stats(0, r)
 
-    late_first = list(range(1, chunks)) + [0]
+    order_conv = [1, 0] + list(range(2, chunks))
     moments, means = {}, {}
-    for r in late_first:
+    for r in order_conv:
         if r == 0:
             @pl.when(me > 0)
             def _():
@@ -264,8 +265,12 @@
     load_wp.wait()
     load_og.wait()
     mix(0)
-    for r in late_first:
+    carry = tuple(jnp.zeros((8, LANES), F32) for _ in range(2 * halves))
+    for r in order_conv[:-1]:
         norm_chunk(r)
+    for r in range(2):
+        means[r], carry = cotangent_chunk(r, carry)
+    norm_chunk(order_conv[-1])
 
     aligned = rows % LANES == 0
     wide = 256
@@ -318,7 +323,18 @@
             far_out.at[j, 0], far_in.at[j, slot], far_send.at[j, 0], far_recv.at[j, slot], {"sp": mate}
         )
 
-    def far_step(j, k):
+    def far_step(j, k, only=None):
+        mask, i = blocks_of[k]
+        if not mask and i < 3 and only != 1:
+            far_copies[j].append(describe(
+                far_out.at[j, i], far_in.at[j, i], far_send.at[j, i], far_recv.at[j, i], {"sp": mate}
+            ))
+        if only is None:
+            far_part(j, k)
+        else:
+            pl.when(edge == only)(lambda: far_part(j, k))
+
+    def far_part(j, k):
         mask, i = blocks_of[k]
         b = device_block(k, inner)
         total = product(j, b) if aligned else part[j, b].astype(F32)
@@ -355,10 +371,10 @@
         else:
             far_out[j, i] = total.astype(BF)
             slot, target = (1 - edge) * 2, place + flip_near
-        far_copies[j].append(send(
+        send(
             far_out.at[j, i], far_in.at[j, slot], far_send.at[j, i], far_recv.at[j, slot],
             {"sp": 2 * outer_of(target, 0) + inner},
-        ))
+        )
 
     def whole(j):
         total = own[j]
@@ -371,10 +387,8 @@
     make_mates(0, pairs[0])
     send_mates(0, pairs[0])
 
-    carry = tuple(jnp.zeros((8, LANES), F32) for _ in range(2 * halves))
-    for r in range(0, chunks, 2):
-        if r:
-            mix(r)
+    for r in range(2, chunks, 2):
+        mix(r)
         for i in (r, r + 1):
             means[i], carry = cotangent_chunk(i, carry)
     for ks in pairs[1:]:
@@ -455,8 +469,7 @@
     for ks in pairs[1:]:
         send_mates(0, ks)
     todo = [(j, k) for j in range(1 + halves) for k in range(h - 1)]
-    for r in range(1, chunks):
-        filtered_chunk(r)
+    filtered_chunk(1)
 
 
     def far_steps(count):
@@ -465,10 +478,12 @@
 
     for c in range(halves):
         back_chunk(0, c)
-    far_steps(1)
     near_block(0)
+    early = group == 1
     for c in range(halves):
         for r in range(1, chunks):
+            if c == 0 and r + 1 < chunks:
+                filtered_chunk(r + 1)
             if c == 0 and r == chunks - 1:
                 @pl.when(me < n - 1)
                 def _():
@@ -476,6 +491,7 @@
             back_chunk(r, c)
             if c == 0 and r == 1:
                 far_block(0)
+                far_steps(1)
             if c == halves - 1:
                 near_block(r)
                 if r > 1:
@@ -501,7 +517,9 @@
         total = whole(1 + c)
         ws_ref[c] = total.T if aligned else total
 
-    far_steps(len(todo) - (h - 1))
+    far_steps(len(todo) - h)
+    late = todo.pop(0)
+    far_step(*late, only=0 if early else None)
     small_copy.wait_recv()
     small_pair[...] = small[inner] + small_in[...]
     small_copies = [
@@ -513,6 +531,8 @@
     total = whole(0)
     ps_ref[...] = total if aligned else total.T
     far_steps(len(todo) - 1)
+    if early:
+        far_step(*late, only=1)
     for copy in small_copies:
         copy.wait_recv()
     small_all[outer] = small_pair[...]

time: 57.4 us -> 56.4 us (0.983)
  Pallas kernels: 56.2 us -> 55.4 us
    pallas_call x1, Pallas kernels: 54.9 us -> 54.1 us  [shards(): pl.pallas_call(functools.partial(main_kernel, n, n_tp, chans * n_tp, halo...]
where the time goes in v4:
time: 56.4 us; the launch traced here: 56.2 us
  Pallas kernels  55.4 us (98%)
  between operations  0.8 us (1%)
    pallas_call x1, Pallas kernels, shards(): pl.pallas_call(functools.partial(main_kernel, n, n_tp, chans * n_tp, halo...  54.1 us
    pallas_call x1, Pallas kernels, shards(): pl.pallas_call(finish_kernel, out_shape=(shape((tokens, cols), BF), shape...  1.3 us

profile of v4, /device:TPU:0, one launch (start us, length us, event | category | flops | bytes accessed | tf_op | source)
XLA Modules:
  0.0 56.2 jit_solution(11996961223534282183)
XLA Ops:
  0.6 54.1 %main.1 = (bf16[1024,512]{1,0:T(8,128)(2,1)S(1)}, f32[2,256,256]{2,1,0:T(8,128)S(1)}, f32[256,256]{1,0:T(8,128)S(1)}, f32[2,40,128]{2,1,0:T(8,128)S(1)}) custom-call(bf16[1024,2048]{1,0:T(8,128)(2,1)} %bi_hbm.1, bf16[1024,2048]{1,0:T(8,128)(2,1)} %og_hbm.1, bf16[2048,256]{1,0:T(8,128)(2,1)} %wv_hbm.1, bf16[2048,256]{1,0:T(8,128)(2,1)} %wg_hbm.1, ...), custom_call_target="tpu_custom_call" | custom-call | tf_op jit(solution)/shard_map/main/pallas_call | solution.py:615
  54.8 1.3 %finish.1 = (bf16[1024,512]{1,0:T(8,128)(2,1)}, f32[256,256]{1,0:T(8,128)}, f32[256,256]{1,0:T(8,128)}, f32[256,256]{1,0:T(8,128)}, f32[31,256]{1,0:T(8,128)}, /*index=5*/f32[1,256]{1,0:T(1,128)}, f32[1,256]{1,0:T(1,128)}) custom-call(bf16[1024,512]{1,0:T(8,128)(2,1)S(1)} %get-tuple-element.18.ig_ref, f32[2,256,256]{2,1,0:T(8,128)S(1)} %get-tuple-element.19.ws_ref, ...), custom_call_target="tpu_custom_call" | custom-call | tf_op jit(solution)/shard_map/finish/pallas_call | solution.py:654
